TPU v7x, 32 devices: a whole 2x2x4 slice. The times are simulated.
32 devices in a mesh: grp: 2 (over y), sp: 4 (over z), tp: 4 (over x, core).
Axes of the slice: x: 2, y: 2, z: 4, core: 2. Of those that a mesh axis runs over, the one named last changes fastest.
Arguments:
- hidden: bfloat16 [3072, 2048], P(('grp', 'sp'), 'tp'), parts along dimension 0, may hold values from -45 to 45
- norm_gain: bfloat16 [2048], replicated, may hold values from 0.099609375 to 1.8984375
- w_query: bfloat16 [2048, 1024], P(None, 'tp'), may hold values from -0.125 to 0.125
- w_key: bfloat16 [2048, 1024], P(None, 'tp'), may hold values from -0.125 to 0.125
- w_value: bfloat16 [2048, 1024], P(None, 'tp'), may hold values from -0.125 to 0.125
- query_gain: float32 [8, 128], P('tp'), may hold values from 0.3 to 16
- key_gain: float32 [8, 128], P('tp'), may hold values from 0.3 to 16
- w_out: bfloat16 [1024, 2048], P('tp'), may hold values from -1.5 to 1.5
Outputs:
- mixed: bfloat16 [3072, 2048], P(('grp', 'sp'), 'tp'), parts along dimension 0
- log_total: float32 [3072, 8], P(('grp', 'sp'), 'tp'), parts along dimension 0
There are 2 independent parts, one for each index of `grp`. A program takes and returns all parts, laid end to end along the dimension named above; an argument that names none is the same for every part. Nothing has to cross between parts.
All inputs are finite; a program needn't handle non-finite values.
Results may differ from a plain program's by a relative error of at most 0.015.
The roundings to bfloat16 on the way count: a program that leaves them out, or rounds other values in their place, can miss the bound.
Values may be sent and summed in bfloat16 or wider, within the bound.
A program may use at most 64 MiB of HBM per device.

v0:
```python
import functools
import math

import jax
import jax.numpy as jnp
import numpy as np
from jax import lax
from jax.experimental import pallas as pl
from jax.experimental.pallas import tpu as pltpu
from jax.sharding import PartitionSpec as P

D = 2048
KEYS_BEHIND = 128
MIDDLE_DILATION = 4
WIDEST_DILATION = 16


EPSILON = 1e-06
ROTARY_BASE = 500000.0


def from_behind(value, axis, steps):
    count = lax.axis_size(axis)
    initial, last = (max(0, -steps), min(count, count - steps))
    return lax.ppermute(value, axis, [(source, source + steps) for source in range(initial, last)])


def rotate(values, positions):
    head_width = values.shape[-1]
    inverse = ROTARY_BASE ** (-jnp.arange(0, head_width, 2, dtype=jnp.float32) / head_width)
    angles = positions[:, None] * inverse[None, :]
    cosine = jnp.cos(angles)[:, None, :]
    sine = jnp.sin(angles)[:, None, :]
    half_width = head_width // 2
    first_half = values[..., :half_width]
    second_half = values[..., half_width:]
    return jnp.concatenate(
        [first_half * cosine - second_half * sine, second_half * cosine + first_half * sine],
        axis=-1,
    )


def head_norm(values, gains):
    normed = values * lax.rsqrt(jnp.mean(values * values, axis=-1, keepdims=True) + EPSILON)
    return normed * gains[None, :, :]


def earlier_pairs(own_pair, token_rows):
    distant_shards = (KEYS_BEHIND * WIDEST_DILATION + token_rows - 1) // token_rows
    pieces = [own_pair]
    for distance in range(1, distant_shards + 1):
        pieces.insert(0, from_behind(own_pair, "sp", distance))
    buffer = jnp.concatenate(pieces, axis=1)
    return buffer


def local_branch(query, key_rows, value_rows, dilation_step, first_pos):
    token_rows, head_count, head_width = query.shape
    reach_rows = KEYS_BEHIND * dilation_step
    buffer_rows = key_rows.shape[0]
    class_rows = token_rows // dilation_step
    class_keys = class_rows + KEYS_BEHIND
    window_start = buffer_rows - token_rows - reach_rows
    key_window = key_rows[window_start:]
    value_window = value_rows[window_start:]
    query_class = query.reshape(class_rows, dilation_step, head_count, head_width).transpose(
        1, 0, 2, 3
    )
    key_class = key_window.reshape(class_keys, dilation_step, head_count, head_width).transpose(
        1, 0, 2, 3
    )
    value_class = value_window.reshape(class_keys, dilation_step, head_count, head_width).transpose(
        1, 0, 2, 3
    )
    block_rows = math.gcd(class_rows, KEYS_BEHIND) if class_rows > KEYS_BEHIND else class_rows
    block_count = class_rows // block_rows
    query_blocks = query_class.reshape(
        dilation_step, block_count, block_rows, head_count, head_width
    )
    key_blocks = jnp.stack(
        [
            key_class[:, number * block_rows : number * block_rows + block_rows + KEYS_BEHIND]
            for number in range(block_count)
        ],
        axis=1,
    )
    value_blocks = jnp.stack(
        [
            value_class[:, number * block_rows : number * block_rows + block_rows + KEYS_BEHIND]
            for number in range(block_count)
        ],
        axis=1,
    )
    scores = jnp.einsum(
        "rnqhd,rnkhd->rnhqk", query_blocks, key_blocks, preferred_element_type=jnp.float32
    ) * head_width ** (-0.5)
    row_index = jnp.arange(block_rows, dtype=jnp.int32)[:, None]
    col_index = jnp.arange(block_rows + KEYS_BEHIND, dtype=jnp.int32)[None, :]
    distance = KEYS_BEHIND + row_index - col_index
    in_band = (distance >= 0) & (distance <= KEYS_BEHIND)
    class_index = jnp.arange(block_count, dtype=jnp.int32)[:, None] * block_rows + col_index
    residue = jnp.arange(dilation_step, dtype=jnp.int32)[:, None, None]
    key_position = first_pos - reach_rows + class_index[None] * dilation_step + residue
    allowed = in_band[None, None, None, :, :] & (key_position >= 0)[:, :, None, None, :]
    scores = jnp.where(allowed, scores, -jnp.inf)
    row_max = jnp.max(scores, axis=-1, keepdims=True)
    weights = jnp.exp(scores - row_max)
    weight_sum = jnp.sum(weights, axis=-1)
    weighted = jnp.einsum(
        "rnhqk,rnkhd->rnqhd",
        weights.astype(jnp.bfloat16),
        value_blocks,
        preferred_element_type=jnp.float32,
    )
    branch_out = weighted / jnp.transpose(weight_sum, (0, 1, 3, 2))[..., None]
    branch_out = branch_out.reshape(dilation_step, class_rows, head_count, head_width).transpose(
        1, 0, 2, 3
    )
    branch_out = branch_out.reshape(token_rows, head_count, head_width)
    log_sum = jnp.transpose(row_max[..., 0] + jnp.log(weight_sum), (0, 1, 3, 2))
    log_sum = (
        log_sum.reshape(dilation_step, class_rows, head_count)
        .transpose(1, 0, 2)
        .reshape(token_rows, head_count)
    )
    return (branch_out, log_sum)


def local(hidden, norm_gain, w_query, w_key, w_value, query_gain, key_gain, w_out):
    token_rows = hidden.shape[0]
    local_width = w_query.shape[1]
    head_count = query_gain.shape[0]
    head_width = query_gain.shape[1]
    gain_full = norm_gain.astype(jnp.float32)
    raw_piece = lax.all_gather(hidden, "tp", axis=1, tiled=True).astype(jnp.float32)
    scaled = (raw_piece * gain_full[None, :]).astype(jnp.bfloat16)

    def add_product(weight):
        return jnp.dot(scaled, weight, preferred_element_type=jnp.float32)

    query_raw = add_product(w_query)
    key_raw = add_product(w_key)
    value_raw = add_product(w_value)
    squares = jnp.sum(raw_piece * raw_piece, axis=1)
    row_scale = lax.rsqrt(squares / D + EPSILON)[:, None]
    first_pos = lax.axis_index("sp") * token_rows
    positions = (jnp.arange(token_rows, dtype=jnp.int32) + first_pos).astype(jnp.float32)
    query = rotate(
        head_norm((query_raw * row_scale).reshape(token_rows, head_count, head_width), query_gain),
        positions,
    ).astype(jnp.bfloat16)
    key_now = rotate(
        head_norm((key_raw * row_scale).reshape(token_rows, head_count, head_width), key_gain),
        positions,
    ).astype(jnp.bfloat16)
    value_now = (value_raw * row_scale).astype(jnp.bfloat16)
    own_pair = jnp.stack([key_now.reshape(token_rows, local_width), value_now], axis=0)
    buffer = earlier_pairs(own_pair, token_rows)
    key_rows = buffer[0].reshape(-1, head_count, head_width)
    value_rows = buffer[1].reshape(-1, head_count, head_width)
    branch_outs = []
    branch_logs = []
    for dilation_step in (1, MIDDLE_DILATION, WIDEST_DILATION):
        branch_out, log_sum = local_branch(query, key_rows, value_rows, dilation_step, first_pos)
        branch_outs.append(branch_out)
        branch_logs.append(log_sum)
    stacked_logs = jnp.stack(branch_logs, axis=0)
    peak = jnp.max(stacked_logs, axis=0)
    log_total = peak + jnp.log(jnp.sum(jnp.exp(stacked_logs - peak[None]), axis=0))
    shares = jnp.exp(stacked_logs - log_total[None])
    attended = jnp.sum(shares[..., None] * jnp.stack(branch_outs, axis=0), axis=0)
    attended = attended.astype(jnp.bfloat16).reshape(token_rows, local_width)
    column_block = lax.all_to_all(w_out, "tp", split_axis=1, concat_axis=0, tiled=True)
    mixed = jnp.dot(
        lax.all_gather(attended, "tp", axis=1, tiled=True),
        column_block,
        preferred_element_type=jnp.float32,
    )
    return (mixed.astype(jnp.bfloat16), log_total)


MESH = pl.DeviceIdType.MESH
LANES = 128


def rotary_table(classes, rows, head_width):
    inverse = (ROTARY_BASE ** (-np.arange(0, head_width, 2, dtype=np.float64) / head_width)).astype(np.float32)
    positions = np.arange(classes * classes * rows, dtype=np.float32)
    angles = (positions[:, None] * inverse[None, :]).astype(np.float64)
    cosine, sine = np.cos(angles), np.sin(angles)
    table = np.concatenate([cosine, cosine, -sine, sine], axis=1).astype(np.float32)
    return table.reshape(classes, rows, classes, 2 * head_width).transpose(0, 2, 1, 3)


def class_kernel(
    hid_ref, gain_ref, qgain_ref, kgain_ref, wq_ref, wk_ref, wv_ref, wo_ref, table_ref,
    mixed_ref, total_ref,
    hid, gain_in, qgain, kgain, hb, hc, wall, wo, tb, tc, acc_b, acc_c, q_b, kv_b, kv_c, q_c,
    halo, oc, lsend, ro, rl, near_out, near_log, all_log, at, gain, drain,
    loc, sent, zr, axr, acr, afr, cxr, ccr, cfr, wor, wfr, hs, hr, rr, lr, gxr, gcr, gfr,
):
    f32, bf16 = jnp.float32, jnp.bfloat16
    g, s, p = lax.axis_index("grp"), lax.axis_index("sp"), lax.axis_index("tp")
    n = MIDDLE_DILATION
    rows, width = hid_ref.shape
    sub = rows // n
    heads, hd = qgain_ref.shape
    lw = heads * hd
    halo_sub = halo.shape[1]
    halo_rows = n * halo_sub
    core = p + 1 - 2 * lax.rem(p, 2)
    xp = lax.rem(p + 2, 4)
    diag = lax.rem(core + 2, 4)
    order = (1, 2, 3)
    block_of = [s, s + 1 - 2 * lax.rem(s, 2), 2 - s // 2, 3 - 3 * (s // 2)]

    def copy_to(axis, src, dst, ss, sr, q):
        return pltpu.make_async_remote_copy(
            src_ref=src, dst_ref=dst, send_sem=ss, recv_sem=sr, device_id={axis: q}, device_id_type=MESH
        )

    tp_copy = functools.partial(copy_to, "tp")
    sp_copy = functools.partial(copy_to, "sp")
    load_hid = pltpu.make_async_copy(hid_ref, hid, loc.at[1])
    load_hid.start()
    barrier = pltpu.get_barrier_semaphore()
    for q in (core, xp, diag):
        pl.semaphore_signal(barrier, inc=1, device_id={"tp": q}, device_id_type=MESH)
    for k in range(1, n):
        pl.semaphore_signal(barrier, inc=1, device_id={"sp": lax.rem(s + k, n)}, device_id_type=MESH)
    pl.semaphore_signal(barrier, inc=1, device_id={"grp": 1 - g}, device_id_type=MESH)
    loads = [
        pltpu.make_async_copy(gain_ref, gain_in, loc.at[0]),
        pltpu.make_async_copy(qgain_ref, qgain, loc.at[2]),
        pltpu.make_async_copy(kgain_ref, kgain, loc.at[3]),
        pltpu.make_async_copy(wq_ref, wall.at[:, pl.ds(0, lw)], loc.at[4]),
        pltpu.make_async_copy(wk_ref, wall.at[:, pl.ds(lw, lw)], loc.at[5]),
        pltpu.make_async_copy(wv_ref, wall.at[:, pl.ds(2 * lw, lw)], loc.at[6]),
        pltpu.make_async_copy(table_ref.at[s], tb, loc.at[7]),
        pltpu.make_async_copy(table_ref.at[:, s], tc, loc.at[8]),
        pltpu.make_async_copy(
            wo_ref.at[:, pl.ds(pl.multiple_of(p * width, LANES), width)], wo.at[p], loc.at[9]
        ),
    ]
    for load in loads:
        load.start()

    def iota(shape, dim):
        return lax.broadcasted_iota(jnp.int32, shape, dim)

    def row_of(r, part):
        return n * lax.rem(r, part) + r // part

    square = (rows, rows)
    to_class = (row_of(iota(square, 0), sub) == iota(square, 1)).astype(f32).astype(bf16)
    load_hid.wait()
    permuted = jnp.dot(to_class, hid[...], preferred_element_type=f32).astype(bf16)
    hb[p] = permuted.reshape(n, sub, width)
    pl.semaphore_wait(barrier, 3 + n)

    sends = []

    def go(copy):
        copy.start()
        sends.append(math.prod(copy.src_ref.shape) * copy.src_ref.dtype.itemsize)
        return copy

    for k in order:
        to = block_of[k]
        go(sp_copy(hb.at[p, to], hc.at[p, s], sent, zr.at[s], to))
    piece_of = [lax.rem(s + k, n) for k in range(n)]
    ax = [go(tp_copy(hb.at[p, i], hb.at[p, i], sent, axr.at[j], xp)) for j, i in enumerate(piece_of)]
    ac = go(tp_copy(hb.at[p], hb.at[p], sent, acr, core))

    cx, cc, cf = {}, {}, {}

    def spread(k):
        piece = hc.at[p, block_of[k]]
        cx[k] = go(tp_copy(piece, piece, sent, cxr.at[k], xp))
        cc[k] = go(tp_copy(piece, piece, sent, ccr.at[k], core))

    for load in loads:
        load.wait()
    flat_gain = gain_in[...].astype(f32)
    for j in range(flat_gain.shape[0]):
        each = width // LANES
        gain[j // each, :, (j % each) * LANES : (j % each + 1) * LANES] = flat_gain[j : j + 1]

    def chunk(raw, q):
        raw = raw.astype(f32)
        scaled = (raw * gain[q]).astype(bf16)
        w = wall[pl.ds(pl.multiple_of(q * width, LANES), width), :]
        return jnp.dot(scaled, w, preferred_element_type=f32), jnp.sum(raw * raw, axis=1, keepdims=True)

    def chunk_b(q):
        return chunk(hb[q].reshape(rows, width), q)

    acc_b[...], sq_b = chunk_b(p)
    ac.wait_recv()
    prod, more = chunk_b(core)
    acc_b[...] += prod
    sq_b += more

    for j, i in enumerate(piece_of):
        ax[j].wait_recv()
        go(tp_copy(hb.at[xp, i], hb.at[xp, i], sent, afr, core))
        if j >= 1:
            source = block_of[order[j - 1]]
            sp_copy(hb.at[p, source], hc.at[p, source], sent, zr.at[source], source).wait_recv()
            spread(order[j - 1])
    half = lw // 2
    mine = pl.ds(pl.multiple_of(g * half, 8), half)
    w_sends = [
        go(tp_copy(wo_ref.at[:, pl.ds(pl.multiple_of(core * width, LANES), width)], wo.at[p], sent, wor.at[0], core))
    ]
    for j, q in ((1, xp), (2, diag)):
        w_sends.append(go(tp_copy(
            wo_ref.at[mine, pl.ds(pl.multiple_of(q * width, LANES), width)], wo.at[p, mine], sent, wor.at[j], q
        )))

    prod, more = chunk_b(xp)
    acc_b[...] += prod
    sq_b += more
    def pieces(ks, q):
        return chunk(jnp.concatenate([hb[q, s] if k == 0 else hc[q, block_of[k]] for k in ks], axis=0), q)

    def close_pieces(ks):
        for k in ks:
            if k != 0:
                cc[k].wait_recv()
        first, squares = pieces(ks, p)
        prod, more = pieces(ks, core)
        return first + prod, squares + more

    def cross(k):
        cx[k].wait_recv()
        piece = hc.at[xp, block_of[k]]
        cf[k] = go(tp_copy(piece, piece, sent, cfr.at[k], core))

    acc_c[0], sq_0 = close_pieces((0, 1))
    cross(1)
    tp_copy(hb.at[diag], hb.at[diag], sent, afr, core).wait_recv()
    prod, more = chunk_b(diag)
    sq_b += more

    def finish(acc, sq, table, put_q, put_kv):
        raw = acc * lax.rsqrt(sq / (width * 4) + EPSILON)
        cosine, sine = table[:, :hd], table[:, hd:]
        for h in range(heads):
            for start, gains, put in ((0, qgain, put_q), (lw, kgain, put_kv)):
                x = raw[:, start + h * hd : start + (h + 1) * hd]
                x = x * lax.rsqrt(jnp.mean(x * x, axis=-1, keepdims=True) + EPSILON)
                x = x * gains[pl.ds(h, 1), :]
                x = x * cosine + pltpu.roll(x, hd // 2, 1) * sine
                put(slice(h * hd, (h + 1) * hd), x.astype(bf16))
        put_kv(slice(lw, 2 * lw), raw[:, 2 * lw :].astype(bf16))

    def put_all(ref):
        def put(cols, x):
            ref[:, :, cols] = x.reshape(n, sub, x.shape[1])
        return put

    def put_block(ref, b):
        def put(cols, x):
            ref[b, :, cols] = x
        return put

    finish(acc_b[...] + prod, sq_b, tb[...].reshape(rows, 2 * hd), put_all(q_b), put_all(kv_b))
    halo_send = sp_copy(kv_b.at[:, pl.ds(sub - halo_sub, halo_sub), :], halo, hs, hr, lax.rem(s + 1, n))

    @pl.when(s < n - 1)
    def _():
        halo_send.start()

    @pl.when(s == 0)
    def _():
        halo[...] = jnp.zeros_like(halo)

    def finish_c(ks, acc, sq):
        prod, more = pieces(ks, diag)
        acc, sq = acc + prod, sq + more
        for j, k in enumerate(ks):
            part, b = slice(j * sub, (j + 1) * sub), block_of[k]
            finish(acc[part], sq[part], tc[b], put_block(q_c, b), put_block(kv_c, b))

    prod, more = pieces((0, 1), xp)
    acc_c[0] += prod
    sq_0 += more
    cf[1].wait_recv()
    finish_c((0, 1), acc_c[0], sq_0)
    cross(2)
    acc_c[1], sq_1 = close_pieces((2, 3))
    cross(3)
    prod, more = pieces((2, 3), xp)
    acc_c[1] += prod
    sq_1 += more
    cf[2].wait_recv()
    cf[3].wait_recv()
    finish_c((2, 3), acc_c[1], sq_1)

    def attend(q, k, v, bias):
        score = lax.dot_general(q, k, (((1,), (1,)), ((), ())), preferred_element_type=f32)
        score = score * hd ** (-0.5) + bias
        top = jnp.max(score, axis=-1, keepdims=True)
        weight = jnp.exp(score - top)
        total = jnp.sum(weight, axis=-1, keepdims=True)
        out = jnp.dot(weight.astype(bf16), v, preferred_element_type=f32) / total
        return out, top + jnp.log(total)

    behind = iota(square, 0) - iota(square, 1)
    stride = WIDEST_DILATION // n
    near = (behind >= 0) & (behind <= KEYS_BEHIND)
    far = (behind >= 0) & (behind <= KEYS_BEHIND * stride) & ((behind + rows * stride) % stride == 0)
    bias_c = jnp.where(
        near & far, math.log(2.0), jnp.where(near | far, 0.0, -jnp.inf)
    ).astype(f32)
    lane = iota((rows, LANES), 1)
    logs = jnp.zeros((rows, LANES), f32)
    for h in range(heads):
        cols = slice(h * hd, (h + 1) * hd)
        vcols = slice(lw + h * hd, lw + (h + 1) * hd)
        out, lse = attend(
            q_c[:, :, cols].reshape(rows, hd), kv_c[:, :, cols].reshape(rows, hd),
            kv_c[:, :, vcols].reshape(rows, hd), bias_c,
        )
        oc[h] = out.astype(bf16).reshape(n, sub, hd)
        logs = jnp.where(lane == h, lse, logs)
        for k in order[::-1]:
            to = block_of[k]
            go(sp_copy(oc.at[h, to], ro.at[s, h], sent, rr.at[s], to))
    pad = LANES - sub
    for b in range(n):
        part = jnp.concatenate([logs[b * sub : (b + 1) * sub], jnp.zeros((pad, LANES), f32)], axis=0)
        lsend[b] = jnp.transpose(part)[:8]
    for k in order[::-1]:
        to = block_of[k]
        go(sp_copy(lsend.at[to], rl.at[s], sent, lr.at[s], to))

    @pl.when(s > 0)
    def _():
        halo_send.wait_recv()

    total_keys = rows + halo_rows
    wide = (rows, total_keys)
    key = iota(wide, 1)
    key_row = jnp.where(key < rows, row_of(key, sub), row_of(key - rows, halo_sub) - halo_rows)
    behind = row_of(iota(wide, 0), sub) - key_row
    ok = (behind >= 0) & (behind <= KEYS_BEHIND) & (key_row + s * rows >= 0)
    bias_b = jnp.where(ok, 0.0, -jnp.inf).astype(f32)
    logs = jnp.zeros((rows, LANES), f32)
    for h in range(heads):
        cols = slice(h * hd, (h + 1) * hd)
        vcols = slice(lw + h * hd, lw + (h + 1) * hd)
        out, lse = attend(
            q_b[:, :, cols].reshape(rows, hd),
            jnp.concatenate([kv_b[:, :, cols].reshape(rows, hd), halo[:, :, cols].reshape(halo_rows, hd)], axis=0),
            jnp.concatenate([kv_b[:, :, vcols].reshape(rows, hd), halo[:, :, vcols].reshape(halo_rows, hd)], axis=0),
            bias_b,
        )
        near_out[h] = out.reshape(n, sub, hd)
        logs = jnp.where(lane == h, lse, logs)
    near_log[...] = logs.reshape(n, sub, LANES)

    gx, gc, gf = {}, {}, {}

    def merge(k):
        b = block_of[k]
        received = lsend[s] if k == 0 else rl[b]
        far_log = jnp.transpose(jnp.concatenate([received, jnp.zeros((LANES - 8, LANES), f32)], axis=0))[:sub]
        logs = jnp.zeros((sub, LANES), f32)
        for h in range(heads):
            lse = near_log[b][:, h : h + 1]
            far_lse = far_log[:, h : h + 1]
            far_out = (oc[h, s] if k == 0 else ro[b, h]).astype(f32)
            top = jnp.maximum(lse, far_lse)
            e_near, e_far = jnp.exp(lse - top), jnp.exp(far_lse - top)
            both = e_near + e_far
            logs = jnp.where(lane[:sub] == h, top + jnp.log(both), logs)
            at[p, b, :, h * hd : (h + 1) * hd] = ((e_near * near_out[h, b] + e_far * far_out) / both).astype(bf16)
        all_log[b] = logs
        piece = at.at[p, b]
        gx[k] = go(tp_copy(piece, piece, sent, gxr.at[k], xp))
        gc[k] = go(tp_copy(piece, piece, sent, gcr, core))

    def forward(k):
        gx[k].wait_recv()
        piece = at.at[xp, block_of[k]]
        gf[k] = go(tp_copy(piece, piece, sent, gfr, core))

    merge(0)
    wf = []
    for j, q in ((1, xp), (2, diag)):
        w_sends[j].wait_recv()
        wf.append(go(copy_to("grp", wo.at[q, mine], wo.at[q, mine], sent, wfr.at[j - 1], 1 - g)))
    for k, ready in zip(order, (None, 0, order[0])):
        b = block_of[k]
        sp_copy(ro.at[b], ro.at[b], sent, rr.at[b], b).wait_recv()
        sp_copy(rl.at[b], rl.at[b], sent, lr.at[b], b).wait_recv()
        merge(k)
        if ready is not None:
            forward(ready)
    from_class = (iota(square, 0) == row_of(iota(square, 1), sub)).astype(f32).astype(bf16)
    logs = all_log[...].reshape(rows, LANES)
    high = logs.astype(bf16)
    rest = logs - high.astype(f32)
    middle = rest.astype(bf16)
    low = (rest - middle.astype(f32)).astype(bf16)
    ordered = sum(jnp.dot(from_class, x, preferred_element_type=f32) for x in (high, middle, low))
    for j in range(rows // LANES):
        block = slice(j * LANES, (j + 1) * LANES)
        total_ref[:, block] = jnp.transpose(ordered[block])[:heads]

    def product(q):
        return jnp.dot(at[q].reshape(rows, lw), wo[q], preferred_element_type=f32)

    result = product(p)
    forward(order[1])
    w_sends[0].wait_recv()
    tp_copy(at.at[core], at.at[core], sent, gcr, core).wait_recv()
    result += product(core)
    for copy in wf:
        copy.wait_recv()
    forward(order[2])
    result += product(xp)
    tp_copy(at.at[diag], at.at[diag], sent, gfr, core).wait_recv()
    result += product(diag)
    mixed_ref[...] = jnp.dot(from_class, result.astype(bf16), preferred_element_type=f32).astype(bf16)
    assert sum(sends) == drain.shape[0] * LANES * 4
    tp_copy(drain, drain, sent, acr, core).wait_send()

    @pl.when(s < n - 1)
    def _():
        halo_send.wait_send()


def local_by_class(hidden, norm_gain, w_query, w_key, w_value, query_gain, key_gain, w_out):
    n = MIDDLE_DILATION
    rows, width = hidden.shape
    heads, hd = query_gain.shape
    lw = heads * hd
    sub = rows // n
    halo_sub = KEYS_BEHIND // n
    bf16, f32 = jnp.bfloat16, jnp.float32
    table = jnp.asarray(rotary_table(n, sub, hd))
    sent_bytes = 2 * (24 * sub * width + 3 * lw * width + 3 * sub * lw + 12 * sub * lw) + 3 * 8 * LANES * 4
    vmem = pl.BlockSpec(memory_space=pltpu.VMEM)
    anyspace = pl.BlockSpec(memory_space=pl.ANY)
    dma = pltpu.SemaphoreType.DMA
    mixed, total = pl.pallas_call(
        class_kernel,
        out_shape=(
            pltpu.VMEM((rows, w_out.shape[1] // 4), bf16),
            pltpu.VMEM((heads, rows), f32),
        ),
        in_specs=[anyspace] * 9,
        out_specs=(vmem, vmem),
        scratch_shapes=[
            pltpu.VMEM((rows, width), bf16),
            pltpu.VMEM((4 * width // LANES, LANES), bf16),
            pltpu.VMEM((heads, hd), f32),
            pltpu.VMEM((heads, hd), f32),
            pltpu.VMEM((4, n, sub, width), bf16),
            pltpu.VMEM((4, n, sub, width), bf16),
            pltpu.VMEM((4 * width, 3 * lw), bf16),
            pltpu.VMEM((4, lw, width), bf16),
            pltpu.VMEM((n, sub, 2 * hd), f32),
            pltpu.VMEM((n, sub, 2 * hd), f32),
            pltpu.VMEM((rows, 3 * lw), f32),
            pltpu.VMEM((2, 2 * sub, 3 * lw), f32),
            pltpu.VMEM((n, sub, lw), bf16),
            pltpu.VMEM((n, sub, 2 * lw), bf16),
            pltpu.VMEM((n, sub, 2 * lw), bf16),
            pltpu.VMEM((n, sub, lw), bf16),
            pltpu.VMEM((n, halo_sub, 2 * lw), bf16),
            pltpu.VMEM((heads, n, sub, hd), bf16),
            pltpu.VMEM((n, 8, LANES), f32),
            pltpu.VMEM((n, heads, sub, hd), bf16),
            pltpu.VMEM((n, 8, LANES), f32),
            pltpu.VMEM((heads, n, sub, hd), f32),
            pltpu.VMEM((n, sub, LANES), f32),
            pltpu.VMEM((n, sub, LANES), f32),
            pltpu.VMEM((4, n, sub, lw), bf16),
            pltpu.VMEM((4, 1, width), f32),
            pltpu.VMEM((sent_bytes // (4 * LANES), LANES), f32),
            dma((10,)), dma, dma((n,)), dma((n,)), dma, dma, dma((n,)), dma((n,)), dma((n,)),
            dma((3,)), dma((2,)), dma, dma, dma((n,)), dma((n,)), dma((n,)), dma, dma,
        ],
        compiler_params=pltpu.CompilerParams(
            collective_id=0, has_side_effects=True, vmem_limit_bytes=60 * 1024 * 1024
        ),
    )(
        hidden, norm_gain.reshape(-1, LANES), query_gain, key_gain,
        w_query, w_key, w_value, w_out, table,
    )
    return mixed, total.T


def solution(mesh):
    split = (mesh.shape["grp"], mesh.shape["sp"], mesh.shape["tp"]) == (2, MIDDLE_DILATION, 4)
    chosen = local_by_class if split else local
    placed = (
        P(("grp", "sp"), "tp"),
        P(),
        P(None, "tp"),
        P(None, "tp"),
        P(None, "tp"),
        P("tp", None),
        P("tp", None),
        P("tp", None),
    )
    return jax.shard_map(
        chosen,
        mesh=mesh,
        in_specs=placed,
        out_specs=(P(("grp", "sp"), "tp"), P(("grp", "sp"), "tp")),
        check_vma=False,
    )
```

profile of v0, /device:TPU:0, one launch (start us, length us, event | category | flops | bytes accessed | tf_op | source)
XLA Modules:
  0.0 38.6 jit_solution(2317533163601098509)
XLA Ops:
  0.6 36.6 %shard_map.104 = (bf16[384,512]{1,0:T(8,128)(2,1)S(1)}, f32[2,384]{1,0:T(2,128)S(1)}) custom-call(bf16[384,512]{1,0:T(8,128)(2,1)} %hid_ref.1, bf16[16,128]{1,0:T(8,128)(2,1)} %bitcast.3, f32[2,128]{1,0:T(2,128)} %qgain_ref.1, f32[2,128]{1,0:T(2,128)} %kgain_ref.1, bf16[2048,256]{1,0:T(8,128)(2,1)} %wq_ref.1, bf16[2048,256]{1,0:T(8,128)(2,1)} %wk_ref.1, ...), custom_call_target="tpu_custom_call" | custom-call | tf_op jit(solution)/shard_map/pallas_call | solution.py:549
  37.2 0.7 %copy.13 = bf16[384,512]{1,0:T(8,128)(2,1)} copy(bf16[384,512]{1,0:T(8,128)(2,1)S(1)} %get-tuple-element.6) | data formatting | bytes 786432
  38.0 0.6 %copy.14 = f32[384,2]{0,1:T(2,128)} copy(f32[384,2]{0,1:T(2,128)S(1)} %bitcast.2) | data formatting | bytes 6144
where the time goes:
time: 38.7 us; the launch traced here: 38.6 us
  Pallas kernels  36.6 us (95%)
  local copies, waits for them, and re-layouts  1.33 us (3%)
  between operations  0.64 us (2%)
    pallas_call x1, Pallas kernels, local_by_class(): pl.pallas_call(class_kernel, out_shape=(pltpu.VMEM((rows, w_out.shape[1]...  36.6 us
    unnamed x2, local copies, waits for them, and re-layouts  1.33 us

commit v1 on v0

--- a/solution.py
+++ b/solution.py
@@ -195,9 +195,9 @@
 def class_kernel(
     hid_ref, gain_ref, qgain_ref, kgain_ref, wq_ref, wk_ref, wv_ref, wo_ref, table_ref,
     mixed_ref, total_ref,
-    hid, gain_in, qgain, kgain, hb, hc, wall, wo, tb, tc, acc_b, acc_c, q_b, kv_b, kv_c, q_c,
+    hid, gain_in, qgain, kgain, hb, hm, wall, wo, tb, tm, acc, acc_m, sq, qkv_b, qkv_c,
     halo, oc, lsend, ro, rl, near_out, near_log, all_log, at, gain, drain,
-    loc, sent, zr, axr, acr, afr, cxr, ccr, cfr, wor, wfr, hs, hr, rr, lr, gxr, gcr, gfr,
+    loc, sent, zr, axr, acr, afr, cxr, ccr, cfr, wor, wfr, qr, hs, hr, rr, lr, gxr, gcr, gfr,
 ):
     f32, bf16 = jnp.float32, jnp.bfloat16
     g, s, p = lax.axis_index("grp"), lax.axis_index("sp"), lax.axis_index("tp")
@@ -206,13 +206,14 @@
     sub = rows // n
     heads, hd = qgain_ref.shape
     lw = heads * hd
-    halo_sub = halo.shape[1]
+    halo_sub = halo.shape[2]
     halo_rows = n * halo_sub
     core = p + 1 - 2 * lax.rem(p, 2)
     xp = lax.rem(p + 2, 4)
     diag = lax.rem(core + 2, 4)
-    order = (1, 2, 3)
-    block_of = [s, s + 1 - 2 * lax.rem(s, 2), 2 - s // 2, 3 - 3 * (s // 2)]
+    pair, two, mirror = s + 1 - 2 * lax.rem(s, 2), lax.rem(s + 2, n), n - 1 - s
+    peer = (s, pair, two, mirror)
+    chunk_order = (two, pair, s, mirror)
 
     def copy_to(axis, src, dst, ss, sr, q):
         return pltpu.make_async_remote_copy(
@@ -221,13 +222,17 @@
 
     tp_copy = functools.partial(copy_to, "tp")
     sp_copy = functools.partial(copy_to, "sp")
+
+    def same(copy, ref, sr, q):
+        return copy(ref, ref, sent, sr, q)
+
     load_hid = pltpu.make_async_copy(hid_ref, hid, loc.at[1])
     load_hid.start()
     barrier = pltpu.get_barrier_semaphore()
-    for q in (core, xp, diag):
+    for k in (3, 2, 1):
+        pl.semaphore_signal(barrier, inc=1, device_id={"sp": peer[k]}, device_id_type=MESH)
+    for q in (xp, diag, core):
         pl.semaphore_signal(barrier, inc=1, device_id={"tp": q}, device_id_type=MESH)
-    for k in range(1, n):
-        pl.semaphore_signal(barrier, inc=1, device_id={"sp": lax.rem(s + k, n)}, device_id_type=MESH)
     pl.semaphore_signal(barrier, inc=1, device_id={"grp": 1 - g}, device_id_type=MESH)
     loads = [
         pltpu.make_async_copy(gain_ref, gain_in, loc.at[0]),
@@ -237,7 +242,7 @@
         pltpu.make_async_copy(wk_ref, wall.at[:, pl.ds(lw, lw)], loc.at[5]),
         pltpu.make_async_copy(wv_ref, wall.at[:, pl.ds(2 * lw, lw)], loc.at[6]),
         pltpu.make_async_copy(table_ref.at[s], tb, loc.at[7]),
-        pltpu.make_async_copy(table_ref.at[:, s], tc, loc.at[8]),
+        pltpu.make_async_copy(table_ref.at[mirror, s], tm, loc.at[8]),
         pltpu.make_async_copy(
             wo_ref.at[:, pl.ds(pl.multiple_of(p * width, LANES), width)], wo.at[p], loc.at[9]
         ),
@@ -265,19 +270,18 @@
         sends.append(math.prod(copy.src_ref.shape) * copy.src_ref.dtype.itemsize)
         return copy
 
-    for k in order:
-        to = block_of[k]
-        go(sp_copy(hb.at[p, to], hc.at[p, s], sent, zr.at[s], to))
-    piece_of = [lax.rem(s + k, n) for k in range(n)]
-    ax = [go(tp_copy(hb.at[p, i], hb.at[p, i], sent, axr.at[j], xp)) for j, i in enumerate(piece_of)]
-    ac = go(tp_copy(hb.at[p], hb.at[p], sent, acr, core))
-
-    cx, cc, cf = {}, {}, {}
-
-    def spread(k):
-        piece = hc.at[p, block_of[k]]
-        cx[k] = go(tp_copy(piece, piece, sent, cxr.at[k], xp))
-        cc[k] = go(tp_copy(piece, piece, sent, ccr.at[k], core))
+    part = sub // 2
+    zs = [
+        go(sp_copy(hb.at[p, mirror, pl.ds(a * part, part), :], hm.at[p, a], sent, zr.at[a], mirror))
+        for a in range(2)
+    ]
+    ax = [same(tp_copy, hb.at[p, c], axr.at[j], xp) for j, c in enumerate(chunk_order)]
+    for copy in ax[:3]:
+        go(copy)
+    ac = go(same(tp_copy, hb.at[p], acr, core))
+    w_sends = [
+        go(tp_copy(wo_ref.at[:, pl.ds(pl.multiple_of(core * width, LANES), width)], wo.at[p], sent, wor.at[0], core))
+    ]
 
     for load in loads:
         load.wait()
@@ -292,111 +296,112 @@
         w = wall[pl.ds(pl.multiple_of(q * width, LANES), width), :]
         return jnp.dot(scaled, w, preferred_element_type=f32), jnp.sum(raw * raw, axis=1, keepdims=True)
 
-    def chunk_b(q):
-        return chunk(hb[q].reshape(rows, width), q)
-
-    acc_b[...], sq_b = chunk_b(p)
+    def add_all(q, first):
+        prod, more = chunk(hb[q].reshape(rows, width), q)
+        prod, more = prod.reshape(n, sub, 3 * lw), more.reshape(n, sub, 1)
+        acc[...] = prod if first else acc[...] + prod
+        sq[...] = more if first else sq[...] + more
+
+    add_all(p, True)
     ac.wait_recv()
-    prod, more = chunk_b(core)
-    acc_b[...] += prod
-    sq_b += more
-
-    for j, i in enumerate(piece_of):
-        ax[j].wait_recv()
-        go(tp_copy(hb.at[xp, i], hb.at[xp, i], sent, afr, core))
-        if j >= 1:
-            source = block_of[order[j - 1]]
-            sp_copy(hb.at[p, source], hc.at[p, source], sent, zr.at[source], source).wait_recv()
-            spread(order[j - 1])
-    half = lw // 2
-    mine = pl.ds(pl.multiple_of(g * half, 8), half)
-    w_sends = [
-        go(tp_copy(wo_ref.at[:, pl.ds(pl.multiple_of(core * width, LANES), width)], wo.at[p], sent, wor.at[0], core))
-    ]
-    for j, q in ((1, xp), (2, diag)):
-        w_sends.append(go(tp_copy(
-            wo_ref.at[mine, pl.ds(pl.multiple_of(q * width, LANES), width)], wo.at[p, mine], sent, wor.at[j], q
-        )))
-
-    prod, more = chunk_b(xp)
-    acc_b[...] += prod
-    sq_b += more
-    def pieces(ks, q):
-        return chunk(jnp.concatenate([hb[q, s] if k == 0 else hc[q, block_of[k]] for k in ks], axis=0), q)
-
-    def close_pieces(ks):
-        for k in ks:
-            if k != 0:
-                cc[k].wait_recv()
-        first, squares = pieces(ks, p)
-        prod, more = pieces(ks, core)
-        return first + prod, squares + more
-
-    def cross(k):
-        cx[k].wait_recv()
-        piece = hc.at[xp, block_of[k]]
-        cf[k] = go(tp_copy(piece, piece, sent, cfr.at[k], core))
-
-    acc_c[0], sq_0 = close_pieces((0, 1))
-    cross(1)
-    tp_copy(hb.at[diag], hb.at[diag], sent, afr, core).wait_recv()
-    prod, more = chunk_b(diag)
-    sq_b += more
-
-    def finish(acc, sq, table, put_q, put_kv):
+    add_all(core, False)
+
+    def finish(acc, sq, table, places):
         raw = acc * lax.rsqrt(sq / (width * 4) + EPSILON)
         cosine, sine = table[:, :hd], table[:, hd:]
         for h in range(heads):
-            for start, gains, put in ((0, qgain, put_q), (lw, kgain, put_kv)):
-                x = raw[:, start + h * hd : start + (h + 1) * hd]
-                x = x * lax.rsqrt(jnp.mean(x * x, axis=-1, keepdims=True) + EPSILON)
-                x = x * gains[pl.ds(h, 1), :]
-                x = x * cosine + pltpu.roll(x, hd // 2, 1) * sine
-                put(slice(h * hd, (h + 1) * hd), x.astype(bf16))
-        put_kv(slice(lw, 2 * lw), raw[:, 2 * lw :].astype(bf16))
-
-    def put_all(ref):
-        def put(cols, x):
-            ref[:, :, cols] = x.reshape(n, sub, x.shape[1])
-        return put
-
-    def put_block(ref, b):
-        def put(cols, x):
-            ref[b, :, cols] = x
-        return put
-
-    finish(acc_b[...] + prod, sq_b, tb[...].reshape(rows, 2 * hd), put_all(q_b), put_all(kv_b))
-    halo_send = sp_copy(kv_b.at[:, pl.ds(sub - halo_sub, halo_sub), :], halo, hs, hr, lax.rem(s + 1, n))
-
-    @pl.when(s < n - 1)
-    def _():
-        halo_send.start()
+            for j, gains in enumerate((qgain, kgain, None)):
+                x = raw[:, j * lw + h * hd : j * lw + (h + 1) * hd]
+                if gains is not None:
+                    x = x * lax.rsqrt(jnp.mean(x * x, axis=-1, keepdims=True) + EPSILON)
+                    x = x * gains[pl.ds(h, 1), :]
+                    x = x * cosine + pltpu.roll(x, hd // 2, 1) * sine
+                for ref, c in places:
+                    ref[c, h, :, j * hd : (j + 1) * hd] = x.astype(bf16)
+
+    def take(j):
+        ax[j].wait_recv()
+        go(same(tp_copy, hb.at[xp, chunk_order[j]], afr.at[j], core))
+
+    def close(j, places, between):
+        c = chunk_order[j]
+        prod, more = chunk(hb[xp, c], xp)
+        between()
+        same(tp_copy, hb.at[diag, c], afr.at[j], core).wait_recv()
+        last, most = chunk(hb[diag, c], diag)
+        finish(acc[c] + prod + last, sq[c] + more + most, tb[c], places)
+
+    cx, cc = {}, {}
+
+    def spread(a):
+        zs[a].wait_recv()
+        cx[a] = go(same(tp_copy, hm.at[p, a], cxr.at[a], xp))
+        cc[a] = go(same(tp_copy, hm.at[p, a], ccr, core))
+
+    def cross(a):
+        cx[a].wait_recv()
+        go(same(tp_copy, hm.at[xp, a], cfr, core))
+
+    def give(k):
+        for h in range(heads):
+            go(sp_copy(qkv_b.at[peer[k], h], qkv_c.at[s, h], sent, qr.at[k - 1, h], peer[k]))
+
+    half = lw // 2
+    mine = pl.ds(pl.multiple_of(g * half, 8), half)
+
+    def spread_last():
+        spread(1)
+        go(ax[3])
+        for j, q in ((1, xp), (2, diag)):
+            w_sends.append(go(tp_copy(
+                wo_ref.at[mine, pl.ds(pl.multiple_of(q * width, LANES), width)], wo.at[p, mine], sent, wor.at[j], q
+            )))
+
+    def add_mirror(q):
+        prod, more = chunk(hm[q].reshape(sub, width), q)
+        return prod, more
+
+    squares = []
+
+    def start_mirror():
+        same(tp_copy, hm.at[core], ccr, core).wait_recv()
+        first, one = add_mirror(p)
+        prod, more = add_mirror(core)
+        acc_m[...] = first + prod
+        squares.append(one + more)
+        cross(0)
+
+    take(0)
+    close(0, ((qkv_b, two),), functools.partial(spread, 0))
+    give(2)
+    take(1)
+    close(1, ((qkv_b, pair),), spread_last)
+    give(1)
+    take(2)
+    close(2, ((qkv_b, s), (qkv_c, s)), start_mirror)
+
+    above = lax.rem(s + 1, n)
+
+    def send_halo(cs):
+        @pl.when(s < n - 1)
+        def _():
+            for c in cs:
+                sp_copy(
+                    qkv_b.at[c, :, pl.ds(sub - halo_sub, halo_sub), pl.ds(hd, 2 * hd)], halo.at[c], hs, hr, above
+                ).start()
+
+    whole_halo = sp_copy(halo, halo, hs, hr, above)
+    send_halo(chunk_order[:3])
 
     @pl.when(s == 0)
     def _():
         halo[...] = jnp.zeros_like(halo)
 
-    def finish_c(ks, acc, sq):
-        prod, more = pieces(ks, diag)
-        acc, sq = acc + prod, sq + more
-        for j, k in enumerate(ks):
-            part, b = slice(j * sub, (j + 1) * sub), block_of[k]
-            finish(acc[part], sq[part], tc[b], put_block(q_c, b), put_block(kv_c, b))
-
-    prod, more = pieces((0, 1), xp)
-    acc_c[0] += prod
-    sq_0 += more
-    cf[1].wait_recv()
-    finish_c((0, 1), acc_c[0], sq_0)
-    cross(2)
-    acc_c[1], sq_1 = close_pieces((2, 3))
-    cross(3)
-    prod, more = pieces((2, 3), xp)
-    acc_c[1] += prod
-    sq_1 += more
-    cf[2].wait_recv()
-    cf[3].wait_recv()
-    finish_c((2, 3), acc_c[1], sq_1)
+    cross(1)
+    prod, more = add_mirror(xp)
+    same(tp_copy, hm.at[diag], cfr, core).wait_recv()
+    last, most = add_mirror(diag)
+    finish(acc_m[...] + prod + last, squares[0] + more + most, tm[...], ((qkv_c, mirror),))
 
     def attend(q, k, v, bias):
         score = lax.dot_general(q, k, (((1,), (1,)), ((), ())), preferred_element_type=f32)
@@ -415,30 +420,43 @@
         near & far, math.log(2.0), jnp.where(near | far, 0.0, -jnp.inf)
     ).astype(f32)
     lane = iota((rows, LANES), 1)
-    logs = jnp.zeros((rows, LANES), f32)
-    for h in range(heads):
-        cols = slice(h * hd, (h + 1) * hd)
-        vcols = slice(lw + h * hd, lw + (h + 1) * hd)
-        out, lse = attend(
-            q_c[:, :, cols].reshape(rows, hd), kv_c[:, :, cols].reshape(rows, hd),
-            kv_c[:, :, vcols].reshape(rows, hd), bias_c,
-        )
+    pad = LANES - sub
+
+    def three(ref, h, count):
+        return [ref[:, h, :, j * hd : (j + 1) * hd].reshape(rows, hd) for j in range(count)]
+
+    def far_head(h):
+        for k in (2, 1):
+            same(sp_copy, qkv_c.at[peer[k], h], qr.at[k - 1, h], peer[k]).wait_recv()
+        out, lse = attend(*three(qkv_c, h, 3), bias_c)
         oc[h] = out.astype(bf16).reshape(n, sub, hd)
-        logs = jnp.where(lane == h, lse, logs)
-        for k in order[::-1]:
-            to = block_of[k]
-            go(sp_copy(oc.at[h, to], ro.at[s, h], sent, rr.at[s], to))
-    pad = LANES - sub
-    for b in range(n):
-        part = jnp.concatenate([logs[b * sub : (b + 1) * sub], jnp.zeros((pad, LANES), f32)], axis=0)
-        lsend[b] = jnp.transpose(part)[:8]
-    for k in order[::-1]:
-        to = block_of[k]
-        go(sp_copy(lsend.at[to], rl.at[s], sent, lr.at[s], to))
+        for k in (3, 2, 1):
+            go(sp_copy(oc.at[h, peer[k]], ro.at[s, h], sent, rr.at[k - 1, h], peer[k]))
+        for b in range(n):
+            column = jnp.broadcast_to(lse[b * sub : (b + 1) * sub], (sub, LANES))
+            lsend[h, b] = jnp.transpose(jnp.concatenate([column, jnp.zeros((pad, LANES), f32)], axis=0))[:8]
+        for k in (3, 2, 1):
+            go(sp_copy(lsend.at[h, peer[k]], rl.at[s, h], sent, lr.at[k - 1, h], peer[k]))
+
+    take(3)
+    far_head(0)
+    close(3, ((qkv_b, mirror),), lambda: None)
+    send_halo(chunk_order[3:])
+    for h in range(1, heads):
+        far_head(h)
+
+    wf = []
+
+    def pass_on(j):
+        q = (xp, diag)[j]
+        w_sends[j + 1].wait_recv()
+        wf.append(go(copy_to("grp", wo.at[q, mine], wo.at[q, mine], sent, wfr.at[j], 1 - g)))
+
+    pass_on(0)
 
     @pl.when(s > 0)
     def _():
-        halo_send.wait_recv()
+        whole_halo.wait_recv()
 
     total_keys = rows + halo_rows
     wide = (rows, total_keys)
@@ -449,56 +467,53 @@
     bias_b = jnp.where(ok, 0.0, -jnp.inf).astype(f32)
     logs = jnp.zeros((rows, LANES), f32)
     for h in range(heads):
-        cols = slice(h * hd, (h + 1) * hd)
-        vcols = slice(lw + h * hd, lw + (h + 1) * hd)
+        q, k, v = three(qkv_b, h, 3)
         out, lse = attend(
-            q_b[:, :, cols].reshape(rows, hd),
-            jnp.concatenate([kv_b[:, :, cols].reshape(rows, hd), halo[:, :, cols].reshape(halo_rows, hd)], axis=0),
-            jnp.concatenate([kv_b[:, :, vcols].reshape(rows, hd), halo[:, :, vcols].reshape(halo_rows, hd)], axis=0),
+            q,
+            jnp.concatenate([k, halo[:, h, :, :hd].reshape(halo_rows, hd)], axis=0),
+            jnp.concatenate([v, halo[:, h, :, hd:].reshape(halo_rows, hd)], axis=0),
             bias_b,
         )
         near_out[h] = out.reshape(n, sub, hd)
         logs = jnp.where(lane == h, lse, logs)
     near_log[...] = logs.reshape(n, sub, LANES)
 
-    gx, gc, gf = {}, {}, {}
-
-    def merge(k):
-        b = block_of[k]
-        received = lsend[s] if k == 0 else rl[b]
-        far_log = jnp.transpose(jnp.concatenate([received, jnp.zeros((LANES - 8, LANES), f32)], axis=0))[:sub]
-        logs = jnp.zeros((sub, LANES), f32)
-        for h in range(heads):
-            lse = near_log[b][:, h : h + 1]
-            far_lse = far_log[:, h : h + 1]
-            far_out = (oc[h, s] if k == 0 else ro[b, h]).astype(f32)
-            top = jnp.maximum(lse, far_lse)
-            e_near, e_far = jnp.exp(lse - top), jnp.exp(far_lse - top)
-            both = e_near + e_far
-            logs = jnp.where(lane[:sub] == h, top + jnp.log(both), logs)
-            at[p, b, :, h * hd : (h + 1) * hd] = ((e_near * near_out[h, b] + e_far * far_out) / both).astype(bf16)
-        all_log[b] = logs
-        piece = at.at[p, b]
-        gx[k] = go(tp_copy(piece, piece, sent, gxr.at[k], xp))
-        gc[k] = go(tp_copy(piece, piece, sent, gcr, core))
-
-    def forward(k):
-        gx[k].wait_recv()
-        piece = at.at[xp, block_of[k]]
-        gf[k] = go(tp_copy(piece, piece, sent, gfr, core))
-
-    merge(0)
-    wf = []
-    for j, q in ((1, xp), (2, diag)):
-        w_sends[j].wait_recv()
-        wf.append(go(copy_to("grp", wo.at[q, mine], wo.at[q, mine], sent, wfr.at[j - 1], 1 - g)))
-    for k, ready in zip(order, (None, 0, order[0])):
-        b = block_of[k]
-        sp_copy(ro.at[b], ro.at[b], sent, rr.at[b], b).wait_recv()
-        sp_copy(rl.at[b], rl.at[b], sent, lr.at[b], b).wait_recv()
-        merge(k)
-        if ready is not None:
-            forward(ready)
+    gx = {}
+
+    def merge(k, h):
+        b = peer[k]
+        received = lsend[h, s] if k == 0 else rl[b, h]
+        far_lse = jnp.transpose(
+            jnp.concatenate([received, jnp.zeros((LANES - 8, LANES), f32)], axis=0)
+        )[:sub, :1]
+        lse = near_log[b][:, h : h + 1]
+        far_out = (oc[h, s] if k == 0 else ro[b, h]).astype(f32)
+        top = jnp.maximum(lse, far_lse)
+        e_near, e_far = jnp.exp(lse - top), jnp.exp(far_lse - top)
+        both = e_near + e_far
+        before = jnp.zeros((sub, LANES), f32) if h == 0 else all_log[b]
+        at[p, b, h] = ((e_near * near_out[h, b] + e_far * far_out) / both).astype(bf16)
+        all_log[b] = jnp.where(lane[:sub] == h, top + jnp.log(both), before)
+
+    def share(k, h, piece):
+        gx[k, h] = go(same(tp_copy, piece, gxr.at[k, h], xp))
+        go(same(tp_copy, piece, gcr, core))
+
+    def forward(k, h):
+        gx[k, h].wait_recv()
+        piece = at.at[xp, peer[k]]
+        go(same(tp_copy, piece if k == 0 else piece.at[h], gfr, core))
+
+    for h in range(heads):
+        merge(0, h)
+    share(0, 0, at.at[p, s])
+    pass_on(1)
+    for h in range(heads):
+        for k in (1, 2, 3):
+            same(sp_copy, ro.at[peer[k], h], rr.at[k - 1, h], peer[k]).wait_recv()
+            same(sp_copy, rl.at[peer[k], h], lr.at[k - 1, h], peer[k]).wait_recv()
+            merge(k, h)
+            share(k, h, at.at[p, peer[k], h])
     from_class = (iota(square, 0) == row_of(iota(square, 1), sub)).astype(f32).astype(bf16)
     logs = all_log[...].reshape(rows, LANES)
     high = logs.astype(bf16)
@@ -511,26 +526,29 @@
         total_ref[:, block] = jnp.transpose(ordered[block])[:heads]
 
     def product(q):
-        return jnp.dot(at[q].reshape(rows, lw), wo[q], preferred_element_type=f32)
+        x = jnp.concatenate([at[q, :, h].reshape(rows, hd) for h in range(heads)], axis=1)
+        return jnp.dot(x, wo[q], preferred_element_type=f32)
 
     result = product(p)
-    forward(order[1])
+    forward(0, 0)
     w_sends[0].wait_recv()
-    tp_copy(at.at[core], at.at[core], sent, gcr, core).wait_recv()
+    same(tp_copy, at.at[core], gcr, core).wait_recv()
     result += product(core)
+    for h in range(heads):
+        for k in (1, 2, 3):
+            forward(k, h)
     for copy in wf:
         copy.wait_recv()
-    forward(order[2])
     result += product(xp)
-    tp_copy(at.at[diag], at.at[diag], sent, gfr, core).wait_recv()
+    same(tp_copy, at.at[diag], gfr, core).wait_recv()
     result += product(diag)
     mixed_ref[...] = jnp.dot(from_class, result.astype(bf16), preferred_element_type=f32).astype(bf16)
     assert sum(sends) == drain.shape[0] * LANES * 4
-    tp_copy(drain, drain, sent, acr, core).wait_send()
+    same(tp_copy, drain, acr, core).wait_send()
 
     @pl.when(s < n - 1)
     def _():
-        halo_send.wait_send()
+        whole_halo.wait_send()
 
 
 def local_by_class(hidden, norm_gain, w_query, w_key, w_value, query_gain, key_gain, w_out):
@@ -542,7 +560,7 @@
     halo_sub = KEYS_BEHIND // n
     bf16, f32 = jnp.bfloat16, jnp.float32
     table = jnp.asarray(rotary_table(n, sub, hd))
-    sent_bytes = 2 * (24 * sub * width + 3 * lw * width + 3 * sub * lw + 12 * sub * lw) + 3 * 8 * LANES * 4
+    sent_bytes = 2 * (16 * sub * width + 3 * lw * width + 21 * sub * lw) + 3 * heads * 8 * LANES * 4
     vmem = pl.BlockSpec(memory_space=pltpu.VMEM)
     anyspace = pl.BlockSpec(memory_space=pl.ANY)
     dma = pltpu.SemaphoreType.DMA
@@ -560,30 +578,30 @@
             pltpu.VMEM((heads, hd), f32),
             pltpu.VMEM((heads, hd), f32),
             pltpu.VMEM((4, n, sub, width), bf16),
-            pltpu.VMEM((4, n, sub, width), bf16),
+            pltpu.VMEM((4, 2, sub // 2, width), bf16),
             pltpu.VMEM((4 * width, 3 * lw), bf16),
             pltpu.VMEM((4, lw, width), bf16),
             pltpu.VMEM((n, sub, 2 * hd), f32),
-            pltpu.VMEM((n, sub, 2 * hd), f32),
-            pltpu.VMEM((rows, 3 * lw), f32),
-            pltpu.VMEM((2, 2 * sub, 3 * lw), f32),
-            pltpu.VMEM((n, sub, lw), bf16),
-            pltpu.VMEM((n, sub, 2 * lw), bf16),
-            pltpu.VMEM((n, sub, 2 * lw), bf16),
-            pltpu.VMEM((n, sub, lw), bf16),
-            pltpu.VMEM((n, halo_sub, 2 * lw), bf16),
+            pltpu.VMEM((sub, 2 * hd), f32),
+            pltpu.VMEM((n, sub, 3 * lw), f32),
+            pltpu.VMEM((sub, 3 * lw), f32),
+            pltpu.VMEM((n, sub, 1), f32),
+            pltpu.VMEM((n, heads, sub, 3 * hd), bf16),
+            pltpu.VMEM((n, heads, sub, 3 * hd), bf16),
+            pltpu.VMEM((n, heads, halo_sub, 2 * hd), bf16),
             pltpu.VMEM((heads, n, sub, hd), bf16),
-            pltpu.VMEM((n, 8, LANES), f32),
+            pltpu.VMEM((heads, n, 8, LANES), f32),
             pltpu.VMEM((n, heads, sub, hd), bf16),
-            pltpu.VMEM((n, 8, LANES), f32),
+            pltpu.VMEM((n, heads, 8, LANES), f32),
             pltpu.VMEM((heads, n, sub, hd), f32),
             pltpu.VMEM((n, sub, LANES), f32),
             pltpu.VMEM((n, sub, LANES), f32),
-            pltpu.VMEM((4, n, sub, lw), bf16),
+            pltpu.VMEM((4, n, heads, sub, hd), bf16),
             pltpu.VMEM((4, 1, width), f32),
             pltpu.VMEM((sent_bytes // (4 * LANES), LANES), f32),
-            dma((10,)), dma, dma((n,)), dma((n,)), dma, dma, dma((n,)), dma((n,)), dma((n,)),
-            dma((3,)), dma((2,)), dma, dma, dma((n,)), dma((n,)), dma((n,)), dma, dma,
+            dma((10,)), dma, dma((2,)), dma((n,)), dma, dma((n,)), dma((2,)), dma, dma,
+            dma((3,)), dma((2,)), dma((2, heads)), dma, dma, dma((3, heads)), dma((3, heads)),
+            dma((n, heads)), dma, dma,
         ],
         compiler_params=pltpu.CompilerParams(
             collective_id=0, has_side_effects=True, vmem_limit_bytes=60 * 1024 * 1024

time: 38.7 us -> 34.2 us (0.88)
  the two profiles are of different devices: /device:TPU:0 before, /device:TPU:21 now
where the time goes in v1:
time: 34.2 us; the launch traced here: 34 us
  Pallas kernels  32.1 us (94%)
  local copies, waits for them, and re-layouts  1.33 us (4%)
  between operations  0.64 us (2%)
    pallas_call x1, Pallas kernels, local_by_class(): pl.pallas_call(class_kernel, out_shape=(pltpu.VMEM((rows, w_out.shape[1]...  32.1 us
    unnamed x2, local copies, waits for them, and re-layouts  1.33 us

profile of v1, /device:TPU:21, one launch (start us, length us, event | category | flops | bytes accessed | tf_op | source)
XLA Modules:
  0.0 34.0 jit_solution(11897822878588669681)
XLA Ops:
  0.6 32.1 %shard_map.104 = (bf16[384,512]{1,0:T(8,128)(2,1)S(1)}, f32[2,384]{1,0:T(2,128)S(1)}) custom-call(bf16[384,512]{1,0:T(8,128)(2,1)} %hid_ref.1, bf16[16,128]{1,0:T(8,128)(2,1)} %bitcast.3, f32[2,128]{1,0:T(2,128)} %qgain_ref.1, f32[2,128]{1,0:T(2,128)} %kgain_ref.1, bf16[2048,256]{1,0:T(8,128)(2,1)} %wq_ref.1, bf16[2048,256]{1,0:T(8,128)(2,1)} %wk_ref.1, ...), custom_call_target="tpu_custom_call" | custom-call | tf_op jit(solution)/shard_map/pallas_call | solution.py:567
  32.7 0.7 %copy.13 = bf16[384,512]{1,0:T(8,128)(2,1)} copy(bf16[384,512]{1,0:T(8,128)(2,1)S(1)} %get-tuple-element.6) | data formatting | bytes 786432
  33.4 0.6 %copy.14 = f32[384,2]{0,1:T(2,128)} copy(f32[384,2]{0,1:T(2,128)S(1)} %bitcast.2) | data formatting | bytes 6144

commit v2 on v1

--- a/solution.py
+++ b/solution.py
@@ -195,9 +195,9 @@
 def class_kernel(
     hid_ref, gain_ref, qgain_ref, kgain_ref, wq_ref, wk_ref, wv_ref, wo_ref, table_ref,
     mixed_ref, total_ref,
-    hid, gain_in, qgain, kgain, hb, hm, wall, wo, tb, tm, acc, acc_m, sq, qkv_b, qkv_c,
-    halo, oc, lsend, ro, rl, near_out, near_log, all_log, at, gain, drain,
-    loc, sent, zr, axr, acr, afr, cxr, ccr, cfr, wor, wfr, qr, hs, hr, rr, lr, gxr, gcr, gfr,
+    hid, gain_in, qgain, kgain, hb, hm, wall, wo, tb, tm, acc, acc_m, sq, q_b, kv_b, q_c, kv_c,
+    halo, oc, lsend, ro, rl, near_out, near_row, halo_out, halo_row, all_log, at, gain, drain,
+    loc, sent, zr, axr, acr, afr, cxr, ccr, cfr, wor, wfr, qr, kr, hr, rr, lr, gxr, gcr, gfr,
 ):
     f32, bf16 = jnp.float32, jnp.bfloat16
     g, s, p = lax.axis_index("grp"), lax.axis_index("sp"), lax.axis_index("tp")
@@ -213,7 +213,8 @@
     diag = lax.rem(core + 2, 4)
     pair, two, mirror = s + 1 - 2 * lax.rem(s, 2), lax.rem(s + 2, n), n - 1 - s
     peer = (s, pair, two, mirror)
-    chunk_order = (two, pair, s, mirror)
+    part = sub // 2
+    pieces = ((two, 0, part), (two, part, part), (pair, 0, sub), (s, 0, sub), (mirror, 0, sub))
 
     def copy_to(axis, src, dst, ss, sr, q):
         return pltpu.make_async_remote_copy(
@@ -270,13 +271,12 @@
         sends.append(math.prod(copy.src_ref.shape) * copy.src_ref.dtype.itemsize)
         return copy
 
-    part = sub // 2
     zs = [
         go(sp_copy(hb.at[p, mirror, pl.ds(a * part, part), :], hm.at[p, a], sent, zr.at[a], mirror))
         for a in range(2)
     ]
-    ax = [same(tp_copy, hb.at[p, c], axr.at[j], xp) for j, c in enumerate(chunk_order)]
-    for copy in ax[:3]:
+    ax = [same(tp_copy, hb.at[p, c, pl.ds(i, m), :], axr.at[j], xp) for j, (c, i, m) in enumerate(pieces)]
+    for copy in ax[:4]:
         go(copy)
     ac = go(same(tp_copy, hb.at[p], acr, core))
     w_sends = [
@@ -306,7 +306,7 @@
     ac.wait_recv()
     add_all(core, False)
 
-    def finish(acc, sq, table, places):
+    def finish(acc, sq, table, places, span):
         raw = acc * lax.rsqrt(sq / (width * 4) + EPSILON)
         cosine, sine = table[:, :hd], table[:, hd:]
         for h in range(heads):
@@ -316,20 +316,25 @@
                     x = x * lax.rsqrt(jnp.mean(x * x, axis=-1, keepdims=True) + EPSILON)
                     x = x * gains[pl.ds(h, 1), :]
                     x = x * cosine + pltpu.roll(x, hd // 2, 1) * sine
-                for ref, c in places:
-                    ref[c, h, :, j * hd : (j + 1) * hd] = x.astype(bf16)
+                for q_ref, kv_ref, c in places:
+                    if j == 0:
+                        q_ref[c, h, span] = x.astype(bf16)
+                    else:
+                        kv_ref[c, h, span, (j - 1) * hd : j * hd] = x.astype(bf16)
 
     def take(j):
+        c, i, m = pieces[j]
         ax[j].wait_recv()
-        go(same(tp_copy, hb.at[xp, chunk_order[j]], afr.at[j], core))
+        go(same(tp_copy, hb.at[xp, c, pl.ds(i, m), :], afr.at[j], core))
 
     def close(j, places, between):
-        c = chunk_order[j]
-        prod, more = chunk(hb[xp, c], xp)
+        c, i, m = pieces[j]
+        span = slice(i, i + m)
+        prod, more = chunk(hb[xp, c, span], xp)
         between()
-        same(tp_copy, hb.at[diag, c], afr.at[j], core).wait_recv()
-        last, most = chunk(hb[diag, c], diag)
-        finish(acc[c] + prod + last, sq[c] + more + most, tb[c], places)
+        same(tp_copy, hb.at[diag, c, pl.ds(i, m), :], afr.at[j], core).wait_recv()
+        last, most = chunk(hb[diag, c, span], diag)
+        finish(acc[c, span] + prod + last, sq[c, span] + more + most, tb[c, span], places, span)
 
     cx, cc = {}, {}
 
@@ -342,16 +347,46 @@
         cx[a].wait_recv()
         go(same(tp_copy, hm.at[xp, a], cfr, core))
 
-    def give(k):
+    parts_of = {1: pieces[2:3], 2: pieces[:2]}
+
+    def class_copy(own, other, sems, k, h, j, arriving):
+        _, i, m = parts_of[k][j]
+        q = peer[k]
+        mine = other.at[q, h, pl.ds(i, m), :]
+        if arriving:
+            return same(sp_copy, mine, sems.at[k - 1, h, j], q)
+        return sp_copy(own.at[q, h, pl.ds(i, m), :], other.at[s, h, pl.ds(i, m), :], sent, sems.at[k - 1, h, j], q)
+
+    kv_copy = functools.partial(class_copy, kv_b, kv_c, kr)
+    q_copy = functools.partial(class_copy, q_b, q_c, qr)
+
+    def give(k, j):
         for h in range(heads):
-            go(sp_copy(qkv_b.at[peer[k], h], qkv_c.at[s, h], sent, qr.at[k - 1, h], peer[k]))
+            @pl.when(s < n - 1)
+            def _():
+                kv_copy(k, h, j, False).start()
+
+            @pl.when(s > 0)
+            def _():
+                q_copy(k, h, j, False).start()
+
+    def receive(k, h):
+        @pl.when(peer[k] < n - 1)
+        def _():
+            for j in range(len(parts_of[k])):
+                kv_copy(k, h, j, True).wait_recv()
+
+        @pl.when(peer[k] > 0)
+        def _():
+            for j in range(len(parts_of[k])):
+                q_copy(k, h, j, True).wait_recv()
 
     half = lw // 2
     mine = pl.ds(pl.multiple_of(g * half, 8), half)
 
     def spread_last():
         spread(1)
-        go(ax[3])
+        go(ax[4])
         for j, q in ((1, xp), (2, diag)):
             w_sends.append(go(tp_copy(
                 wo_ref.at[mine, pl.ds(pl.multiple_of(q * width, LANES), width)], wo.at[p, mine], sent, wor.at[j], q
@@ -372,36 +407,36 @@
         cross(0)
 
     take(0)
-    close(0, ((qkv_b, two),), functools.partial(spread, 0))
-    give(2)
+    close(0, ((q_b, kv_b, two),), lambda: None)
+    give(2, 0)
     take(1)
-    close(1, ((qkv_b, pair),), spread_last)
-    give(1)
+    close(1, ((q_b, kv_b, two),), functools.partial(spread, 0))
+    give(2, 1)
     take(2)
-    close(2, ((qkv_b, s), (qkv_c, s)), start_mirror)
+    close(2, ((q_b, kv_b, pair),), spread_last)
+    give(1, 0)
+    take(3)
+    close(3, ((q_b, kv_b, s), (q_c, kv_c, s)), start_mirror)
 
     above = lax.rem(s + 1, n)
 
-    def send_halo(cs):
-        @pl.when(s < n - 1)
-        def _():
-            for c in cs:
-                sp_copy(
-                    qkv_b.at[c, :, pl.ds(sub - halo_sub, halo_sub), pl.ds(hd, 2 * hd)], halo.at[c], hs, hr, above
-                ).start()
-
-    whole_halo = sp_copy(halo, halo, hs, hr, above)
-    send_halo(chunk_order[:3])
-
-    @pl.when(s == 0)
+    def send_halo(c):
+        sp_copy(kv_b.at[c, :, pl.ds(sub - halo_sub, halo_sub), :], halo.at[c], sent, hr, above).start()
+
+    @pl.when(s < n - 1)
     def _():
-        halo[...] = jnp.zeros_like(halo)
+        send_halo(two)
+        send_halo(s)
+
+    @pl.when(s == 1)
+    def _():
+        send_halo(pair)
 
     cross(1)
     prod, more = add_mirror(xp)
     same(tp_copy, hm.at[diag], cfr, core).wait_recv()
     last, most = add_mirror(diag)
-    finish(acc_m[...] + prod + last, squares[0] + more + most, tm[...], ((qkv_c, mirror),))
+    finish(acc_m[...] + prod + last, squares[0] + more + most, tm[...], ((q_c, kv_c, mirror),), slice(0, sub))
 
     def attend(q, k, v, bias):
         score = lax.dot_general(q, k, (((1,), (1,)), ((), ())), preferred_element_type=f32)
@@ -412,36 +447,58 @@
         out = jnp.dot(weight.astype(bf16), v, preferred_element_type=f32) / total
         return out, top + jnp.log(total)
 
-    behind = iota(square, 0) - iota(square, 1)
+    def log_count(*read):
+        count = sum(each.astype(f32) for each in read)
+        bias = jnp.where(count == 2, math.log(2.0), jnp.where(count == 3, math.log(3.0), 0.0))
+        return jnp.where(count == 0, -jnp.inf, bias)
+
+    def strided(behind, step):
+        return (behind >= 0) & (behind <= KEYS_BEHIND * step) & ((behind + rows * step) % step == 0)
+
+    later = (rows - sub, rows - sub)
+    late, early = iota(later, 0) + sub, iota(later, 1)
     stride = WIDEST_DILATION // n
-    near = (behind >= 0) & (behind <= KEYS_BEHIND)
-    far = (behind >= 0) & (behind <= KEYS_BEHIND * stride) & ((behind + rows * stride) % stride == 0)
-    bias_c = jnp.where(
-        near & far, math.log(2.0), jnp.where(near | far, 0.0, -jnp.inf)
-    ).astype(f32)
+    crosses = late // sub > early // sub
+    bias_c = log_count(strided(late - early, 1) & crosses, strided(late - early, stride) & crosses)
     lane = iota((rows, LANES), 1)
-    pad = LANES - sub
-
-    def three(ref, h, count):
-        return [ref[:, h, :, j * hd : (j + 1) * hd].reshape(rows, hd) for j in range(count)]
+
+    def as_rows(columns):
+        spread_out = jnp.full((sub, LANES), -jnp.inf, f32)
+        for c, column in enumerate(columns):
+            if column is not None:
+                spread_out = jnp.where(lane[:sub] == c, column, spread_out)
+        pad = jnp.zeros((LANES - sub, LANES), f32)
+        return jnp.transpose(jnp.concatenate([spread_out, pad], axis=0))[:8]
+
+    def flat(x):
+        return x.reshape(x.shape[0] * x.shape[1], x.shape[2])
 
     def far_head(h):
-        for k in (2, 1):
-            same(sp_copy, qkv_c.at[peer[k], h], qr.at[k - 1, h], peer[k]).wait_recv()
-        out, lse = attend(*three(qkv_c, h, 3), bias_c)
-        oc[h] = out.astype(bf16).reshape(n, sub, hd)
+        receive(2, h)
+        receive(1, h)
+        out, lse = attend(
+            flat(q_c[1:, h]), flat(kv_c[: n - 1, h, :, :hd]), flat(kv_c[: n - 1, h, :, hd:]), bias_c
+        )
+        oc[h, 1:] = out.astype(bf16).reshape(n - 1, sub, hd)
         for k in (3, 2, 1):
-            go(sp_copy(oc.at[h, peer[k]], ro.at[s, h], sent, rr.at[k - 1, h], peer[k]))
-        for b in range(n):
-            column = jnp.broadcast_to(lse[b * sub : (b + 1) * sub], (sub, LANES))
-            lsend[h, b] = jnp.transpose(jnp.concatenate([column, jnp.zeros((pad, LANES), f32)], axis=0))[:8]
+            @pl.when(peer[k] > 0)
+            def _():
+                sp_copy(oc.at[h, peer[k]], ro.at[s, h], sent, rr.at[k - 1, h], peer[k]).start()
+        lsend[h] = as_rows([None] + [lse[b * sub : (b + 1) * sub] for b in range(n - 1)])
+        rl[s, h] = lsend[h]
         for k in (3, 2, 1):
-            go(sp_copy(lsend.at[h, peer[k]], rl.at[s, h], sent, lr.at[k - 1, h], peer[k]))
-
-    take(3)
+            @pl.when(peer[k] > 0)
+            def _():
+                sp_copy(lsend.at[h], rl.at[s, h], sent, lr.at[k - 1, h], peer[k]).start()
+
     far_head(0)
-    close(3, ((qkv_b, mirror),), lambda: None)
-    send_halo(chunk_order[3:])
+    take(4)
+    close(4, ((q_b, kv_b, mirror),), lambda: None)
+
+    @pl.when((s < n - 1) & (s != 1))
+    def _():
+        send_halo(mirror)
+
     for h in range(1, heads):
         far_head(h)
 
@@ -454,101 +511,134 @@
 
     pass_on(0)
 
+    behind = row_of(iota(square, 0), sub) - row_of(iota(square, 1), sub)
+    bias_b = log_count(*(strided(behind, step) for step in (1, n, WIDEST_DILATION)))
+    gx = [same(tp_copy, at.at[p, h], gxr.at[h], xp) for h in range(heads)]
+    gc = [same(tp_copy, at.at[p, h], gcr, core) for h in range(heads)]
+
+    def share(h):
+        gx[h].start()
+        gc[h].start()
+
+    for h in range(heads):
+        out, lse = attend(flat(q_b[:, h]), flat(kv_b[:, h, :, :hd]), flat(kv_b[:, h, :, hd:]), bias_b)
+        near_out[h] = out.reshape(n, sub, hd)
+        near_row[h] = as_rows([lse[c * sub : (c + 1) * sub] for c in range(n)])
+
+        @pl.when(s == 0)
+        def _():
+            at[p, h] = near_out[h].astype(bf16)
+            share(h)
+            all_log[h] = near_row[h]
+
     @pl.when(s > 0)
     def _():
-        whole_halo.wait_recv()
-
-    total_keys = rows + halo_rows
-    wide = (rows, total_keys)
-    key = iota(wide, 1)
-    key_row = jnp.where(key < rows, row_of(key, sub), row_of(key - rows, halo_sub) - halo_rows)
-    behind = row_of(iota(wide, 0), sub) - key_row
-    ok = (behind >= 0) & (behind <= KEYS_BEHIND) & (key_row + s * rows >= 0)
-    bias_b = jnp.where(ok, 0.0, -jnp.inf).astype(f32)
-    logs = jnp.zeros((rows, LANES), f32)
-    for h in range(heads):
-        q, k, v = three(qkv_b, h, 3)
-        out, lse = attend(
-            q,
-            jnp.concatenate([k, halo[:, h, :, :hd].reshape(halo_rows, hd)], axis=0),
-            jnp.concatenate([v, halo[:, h, :, hd:].reshape(halo_rows, hd)], axis=0),
-            bias_b,
-        )
-        near_out[h] = out.reshape(n, sub, hd)
-        logs = jnp.where(lane == h, lse, logs)
-    near_log[...] = logs.reshape(n, sub, LANES)
-
-    gx = {}
-
-    def merge(k, h):
-        b = peer[k]
-        received = lsend[h, s] if k == 0 else rl[b, h]
-        far_lse = jnp.transpose(
-            jnp.concatenate([received, jnp.zeros((LANES - 8, LANES), f32)], axis=0)
-        )[:sub, :1]
-        lse = near_log[b][:, h : h + 1]
-        far_out = (oc[h, s] if k == 0 else ro[b, h]).astype(f32)
-        top = jnp.maximum(lse, far_lse)
-        e_near, e_far = jnp.exp(lse - top), jnp.exp(far_lse - top)
-        both = e_near + e_far
-        before = jnp.zeros((sub, LANES), f32) if h == 0 else all_log[b]
-        at[p, b, h] = ((e_near * near_out[h, b] + e_far * far_out) / both).astype(bf16)
-        all_log[b] = jnp.where(lane[:sub] == h, top + jnp.log(both), before)
-
-    def share(k, h, piece):
-        gx[k, h] = go(same(tp_copy, piece, gxr.at[k, h], xp))
-        go(same(tp_copy, piece, gcr, core))
-
-    def forward(k, h):
-        gx[k, h].wait_recv()
-        piece = at.at[xp, peer[k]]
-        go(same(tp_copy, piece if k == 0 else piece.at[h], gfr, core))
-
-    for h in range(heads):
-        merge(0, h)
-    share(0, 0, at.at[p, s])
+        sp_copy(halo.at[pl.ds(0, n - 1)], halo.at[pl.ds(0, n - 1)], sent, hr, above).wait_recv()
+        halo[s] = kv_c[s - 1, :, sub - halo_sub :, :]
+        small = (halo_rows, halo_rows)
+        behind = row_of(iota(small, 0), halo_sub) - row_of(iota(small, 1), halo_sub) + halo_rows
+        bias_h = jnp.where(behind <= KEYS_BEHIND, 0.0, -jnp.inf).astype(f32)
+        for h in range(heads):
+            out, lse = attend(
+                flat(q_b[:, h, :halo_sub]), flat(halo[:, h, :, :hd]), flat(halo[:, h, :, hd:]), bias_h
+            )
+            halo_out[h] = out.reshape(n, halo_sub, hd)
+            pad = jnp.full((sub - halo_sub, 1), -jnp.inf, f32)
+            halo_row[h] = as_rows([
+                jnp.concatenate([lse[c * halo_sub : (c + 1) * halo_sub], pad], axis=0) for c in range(n)
+            ])
+
     pass_on(1)
-    for h in range(heads):
-        for k in (1, 2, 3):
-            same(sp_copy, ro.at[peer[k], h], rr.at[k - 1, h], peer[k]).wait_recv()
-            same(sp_copy, rl.at[peer[k], h], lr.at[k - 1, h], peer[k]).wait_recv()
-            merge(k, h)
-            share(k, h, at.at[p, peer[k], h])
+
+    @pl.when(s > 0)
+    def _():
+        for h in range(heads):
+            for k in (1, 2, 3):
+                same(sp_copy, ro.at[peer[k], h], rr.at[k - 1, h], peer[k]).wait_recv()
+                same(sp_copy, rl.at[peer[k], h], lr.at[k - 1, h], peer[k]).wait_recv()
+            ro[s, h] = oc[h, s]
+            which = iota((8, LANES), 0)
+            far_row = jnp.full((8, LANES), -jnp.inf, f32)
+            for c in range(n):
+                far_row = jnp.where(which == c, rl[c, h, pl.ds(s, 1), :], far_row)
+            own, low = near_row[h], halo_row[h]
+            live = (which < n) & (iota((8, LANES), 1) < sub)
+            top = jnp.where(live, jnp.maximum(jnp.maximum(own, low), far_row), 0.0)
+            exps = [jnp.where(live, jnp.exp(x - top), 0.0) for x in (own, low, far_row)]
+            both = jnp.where(live, exps[0] + exps[1] + exps[2], 1.0)
+            all_log[h] = top + jnp.log(both)
+            shares = [x / both for x in exps]
+            columns = jnp.transpose(jnp.concatenate(shares + [jnp.zeros((LANES - 24, LANES), f32)], axis=0))[:sub]
+            for c in range(n):
+                own_part = columns[:, c : c + 1] * near_out[h, c]
+                far_part = columns[:, 16 + c : 17 + c] * ro[c, h].astype(f32)
+                low_part = columns[:halo_sub, 8 + c : 9 + c] * halo_out[h, c]
+                sums = own_part + far_part
+                sums = jnp.concatenate([sums[:halo_sub] + low_part, sums[halo_sub:]], axis=0)
+                at[p, h, c] = sums.astype(bf16)
+            share(h)
+
     from_class = (iota(square, 0) == row_of(iota(square, 1), sub)).astype(f32).astype(bf16)
-    logs = all_log[...].reshape(rows, LANES)
+    def product(q):
+        x = jnp.concatenate([flat(at[q, h]) for h in range(heads)], axis=1)
+        return jnp.dot(x, wo[q], preferred_element_type=f32)
+
+    def forward(h):
+        gx[h].wait_recv()
+        go(same(tp_copy, at.at[xp, h], gfr, core))
+
+    by_head = iota((8, LANES), 0)
+    logs = []
+    for c in range(n):
+        row = jnp.zeros((8, LANES), f32)
+        for h in range(heads):
+            row = jnp.where(by_head == h, all_log[h, c : c + 1, :], row)
+        logs.append(row)
+    logs = jnp.concatenate(logs, axis=1)
+    placed = (n * LANES, rows)
+    to_order = (
+        (n * lax.rem(iota(placed, 0), LANES) + iota(placed, 0) // LANES == iota(placed, 1))
+        & (lax.rem(iota(placed, 0), LANES) < sub)
+    ).astype(f32).astype(bf16)
     high = logs.astype(bf16)
     rest = logs - high.astype(f32)
     middle = rest.astype(bf16)
     low = (rest - middle.astype(f32)).astype(bf16)
-    ordered = sum(jnp.dot(from_class, x, preferred_element_type=f32) for x in (high, middle, low))
-    for j in range(rows // LANES):
-        block = slice(j * LANES, (j + 1) * LANES)
-        total_ref[:, block] = jnp.transpose(ordered[block])[:heads]
-
-    def product(q):
-        x = jnp.concatenate([at[q, :, h].reshape(rows, hd) for h in range(heads)], axis=1)
-        return jnp.dot(x, wo[q], preferred_element_type=f32)
+    total = sum(jnp.dot(x, to_order, preferred_element_type=f32) for x in (high, middle, low))
+    total_ref[...] = total[:heads]
 
     result = product(p)
-    forward(0, 0)
+    forward(0)
     w_sends[0].wait_recv()
     same(tp_copy, at.at[core], gcr, core).wait_recv()
     result += product(core)
-    for h in range(heads):
-        for k in (1, 2, 3):
-            forward(k, h)
+    for h in range(1, heads):
+        forward(h)
     for copy in wf:
         copy.wait_recv()
     result += product(xp)
     same(tp_copy, at.at[diag], gfr, core).wait_recv()
     result += product(diag)
     mixed_ref[...] = jnp.dot(from_class, result.astype(bf16), preferred_element_type=f32).astype(bf16)
-    assert sum(sends) == drain.shape[0] * LANES * 4
-    same(tp_copy, drain, acr, core).wait_send()
-
-    @pl.when(s < n - 1)
+    back = heads * (sub * hd * 2 + 8 * LANES * 4)
+    q_bytes, kv_bytes = 2 * heads * sub * hd * 2, 2 * heads * sub * 2 * hd * 2
+    halo_bytes = (n - 1) * heads * halo_sub * 2 * hd * 2
+    at_bytes = 2 * rows * lw * 2
+
+    def all_sent(total):
+        same(tp_copy, drain.at[pl.ds(0, total // (LANES * 4))], acr, core).wait_send()
+
+    @pl.when(s == 0)
     def _():
-        whole_halo.wait_send()
+        all_sent(sum(sends) + at_bytes + kv_bytes + halo_bytes + 3 * back)
+
+    @pl.when((s > 0) & (s < n - 1))
+    def _():
+        all_sent(sum(sends) + at_bytes + q_bytes + kv_bytes + halo_bytes + 2 * back)
+
+    @pl.when(s == n - 1)
+    def _():
+        all_sent(sum(sends) + at_bytes + q_bytes + 2 * back)
 
 
 def local_by_class(hidden, norm_gain, w_query, w_key, w_value, query_gain, key_gain, w_out):
@@ -560,7 +650,7 @@
     halo_sub = KEYS_BEHIND // n
     bf16, f32 = jnp.bfloat16, jnp.float32
     table = jnp.asarray(rotary_table(n, sub, hd))
-    sent_bytes = 2 * (16 * sub * width + 3 * lw * width + 21 * sub * lw) + 3 * heads * 8 * LANES * 4
+    most_bytes = 2 * (16 * sub * width + 3 * lw * width + 30 * sub * lw) + 3 * heads * 8 * LANES * 4
     vmem = pl.BlockSpec(memory_space=pltpu.VMEM)
     anyspace = pl.BlockSpec(memory_space=pl.ANY)
     dma = pltpu.SemaphoreType.DMA
@@ -586,22 +676,26 @@
             pltpu.VMEM((n, sub, 3 * lw), f32),
             pltpu.VMEM((sub, 3 * lw), f32),
             pltpu.VMEM((n, sub, 1), f32),
-            pltpu.VMEM((n, heads, sub, 3 * hd), bf16),
-            pltpu.VMEM((n, heads, sub, 3 * hd), bf16),
+            pltpu.VMEM((n, heads, sub, hd), bf16),
+            pltpu.VMEM((n, heads, sub, 2 * hd), bf16),
+            pltpu.VMEM((n, heads, sub, hd), bf16),
+            pltpu.VMEM((n, heads, sub, 2 * hd), bf16),
             pltpu.VMEM((n, heads, halo_sub, 2 * hd), bf16),
             pltpu.VMEM((heads, n, sub, hd), bf16),
-            pltpu.VMEM((heads, n, 8, LANES), f32),
+            pltpu.VMEM((heads, 8, LANES), f32),
             pltpu.VMEM((n, heads, sub, hd), bf16),
             pltpu.VMEM((n, heads, 8, LANES), f32),
             pltpu.VMEM((heads, n, sub, hd), f32),
-            pltpu.VMEM((n, sub, LANES), f32),
-            pltpu.VMEM((n, sub, LANES), f32),
-            pltpu.VMEM((4, n, heads, sub, hd), bf16),
+            pltpu.VMEM((heads, 8, LANES), f32),
+            pltpu.VMEM((heads, n, halo_sub, hd), f32),
+            pltpu.VMEM((heads, 8, LANES), f32),
+            pltpu.VMEM((heads, 8, LANES), f32),
+            pltpu.VMEM((4, heads, n, sub, hd), bf16),
             pltpu.VMEM((4, 1, width), f32),
-            pltpu.VMEM((sent_bytes // (4 * LANES), LANES), f32),
-            dma((10,)), dma, dma((2,)), dma((n,)), dma, dma((n,)), dma((2,)), dma, dma,
-            dma((3,)), dma((2,)), dma((2, heads)), dma, dma, dma((3, heads)), dma((3, heads)),
-            dma((n, heads)), dma, dma,
+            pltpu.VMEM((most_bytes // (4 * LANES), LANES), f32),
+            dma((10,)), dma, dma((2,)), dma((n + 1,)), dma, dma((n + 1,)), dma((2,)), dma, dma,
+            dma((3,)), dma((2,)), dma((2, heads, 2)), dma((2, heads, 2)), dma, dma((3, heads)), dma((3, heads)),
+            dma((heads,)), dma, dma,
         ],
         compiler_params=pltpu.CompilerParams(
             collective_id=0, has_side_effects=True, vmem_limit_bytes=60 * 1024 * 1024

time: 34.2 us -> 33.8 us (0.988)
  the two profiles are of different devices: /device:TPU:21 before, /device:TPU:31 now
where the time goes in v2:
time: 33.8 us; the launch traced here: 33.6 us
  Pallas kernels  31.7 us (94%)
  local copies, waits for them, and re-layouts  1.33 us (4%)
  between operations  0.64 us (2%)
    pallas_call x1, Pallas kernels, local_by_class(): pl.pallas_call(class_kernel, out_shape=(pltpu.VMEM((rows, w_out.shape[1]...  31.7 us
    unnamed x2, local copies, waits for them, and re-layouts  1.33 us

profile of v2, /device:TPU:31, one launch (start us, length us, event | category | flops | bytes accessed | tf_op | source)
XLA Modules:
  0.0 33.6 jit_solution(1227343272018028319)
XLA Ops:
  0.6 31.7 %shard_map.104 = (bf16[384,512]{1,0:T(8,128)(2,1)S(1)}, f32[2,384]{1,0:T(2,128)S(1)}) custom-call(bf16[384,512]{1,0:T(8,128)(2,1)} %hid_ref.1, bf16[16,128]{1,0:T(8,128)(2,1)} %bitcast.3, f32[2,128]{1,0:T(2,128)} %qgain_ref.1, f32[2,128]{1,0:T(2,128)} %kgain_ref.1, bf16[2048,256]{1,0:T(8,128)(2,1)} %wq_ref.1, bf16[2048,256]{1,0:T(8,128)(2,1)} %wk_ref.1, ...), custom_call_target="tpu_custom_call" | custom-call | tf_op jit(solution)/shard_map/pallas_call | solution.py:657
  32.3 0.7 %copy.13 = bf16[384,512]{1,0:T(8,128)(2,1)} copy(bf16[384,512]{1,0:T(8,128)(2,1)S(1)} %get-tuple-element.6) | data formatting | bytes 786432
  33.1 0.6 %copy.14 = f32[384,2]{0,1:T(2,128)} copy(f32[384,2]{0,1:T(2,128)S(1)} %bitcast.2) | data formatting | bytes 6144

commit v3 on v2

--- a/solution.py
+++ b/solution.py
@@ -196,8 +196,8 @@
     hid_ref, gain_ref, qgain_ref, kgain_ref, wq_ref, wk_ref, wv_ref, wo_ref, table_ref,
     mixed_ref, total_ref,
     hid, gain_in, qgain, kgain, hb, hm, wall, wo, tb, tm, acc, acc_m, sq, q_b, kv_b, q_c, kv_c,
-    halo, oc, lsend, ro, rl, near_out, near_row, halo_out, halo_row, all_log, at, gain, drain,
-    loc, sent, zr, axr, acr, afr, cxr, ccr, cfr, wor, wfr, qr, kr, hr, rr, lr, gxr, gcr, gfr,
+    halo, oc, lsend, ro, rl, near_out, near_row, halo_out, halo_row, all_log, at, at_own, bias_far, bias_near, gain, drain,
+    loc, sent, zr, axr, acr, afr, cxr, ccr, cfr, wor, wfr, qr, kr, hr, rr, lr, gxr, gcr, gfr, gor, gpr,
 ):
     f32, bf16 = jnp.float32, jnp.bfloat16
     g, s, p = lax.axis_index("grp"), lax.axis_index("sp"), lax.axis_index("tp")
@@ -214,7 +214,9 @@
     pair, two, mirror = s + 1 - 2 * lax.rem(s, 2), lax.rem(s + 2, n), n - 1 - s
     peer = (s, pair, two, mirror)
     part = sub // 2
-    pieces = ((two, 0, part), (two, part, part), (pair, 0, sub), (s, 0, sub), (mirror, 0, sub))
+    pieces = (
+        (two, 0, part), (two, part, part), (pair, 0, sub), (s, 0, sub), (mirror, sub - halo_sub, halo_sub), (mirror, 0, sub - halo_sub)
+    )
 
     def copy_to(axis, src, dst, ss, sr, q):
         return pltpu.make_async_remote_copy(
@@ -381,16 +383,25 @@
             for j in range(len(parts_of[k])):
                 q_copy(k, h, j, True).wait_recv()
 
-    half = lw // 2
-    mine = pl.ds(pl.multiple_of(g * half, 8), half)
+    quarter = lw // 4
+
+    def quarter_of(a):
+        return pl.ds(pl.multiple_of((2 * g + a) * quarter, 8), quarter)
+
+    def spread_first():
+        spread(0)
+        go(ax[4])
 
     def spread_last():
         spread(1)
-        go(ax[4])
-        for j, q in ((1, xp), (2, diag)):
-            w_sends.append(go(tp_copy(
-                wo_ref.at[mine, pl.ds(pl.multiple_of(q * width, LANES), width)], wo.at[p, mine], sent, wor.at[j], q
-            )))
+        go(ax[5])
+        for j, q in ((0, xp), (1, diag)):
+            for a in range(2):
+                block = quarter_of(a)
+                w_sends.append(go(tp_copy(
+                    wo_ref.at[block, pl.ds(pl.multiple_of(q * width, LANES), width)], wo.at[p, block],
+                    sent, wor.at[1 + 2 * j + a], q,
+                )))
 
     def add_mirror(q):
         prod, more = chunk(hm[q].reshape(sub, width), q)
@@ -406,11 +417,26 @@
         squares.append(one + more)
         cross(0)
 
+    def log_count(*read):
+        count = sum(each.astype(f32) for each in read)
+        bias = jnp.where(count == 2, math.log(2.0), jnp.where(count == 3, math.log(3.0), 0.0))
+        return jnp.where(count == 0, -jnp.inf, bias)
+
+    def strided(behind, step):
+        return (behind >= 0) & (behind <= KEYS_BEHIND * step) & ((behind + rows * step) % step == 0)
+
+    later = (rows - sub, rows - sub)
+    late, early = iota(later, 0) + sub, iota(later, 1)
+    stride = WIDEST_DILATION // n
+    crosses = late // sub > early // sub
+    bias_far[...] = log_count(strided(late - early, 1) & crosses, strided(late - early, stride) & crosses)
+    behind = row_of(iota(square, 0), sub) - row_of(iota(square, 1), sub)
+    bias_near[...] = log_count(*(strided(behind, step) for step in (1, n, WIDEST_DILATION)))
     take(0)
     close(0, ((q_b, kv_b, two),), lambda: None)
     give(2, 0)
     take(1)
-    close(1, ((q_b, kv_b, two),), functools.partial(spread, 0))
+    close(1, ((q_b, kv_b, two),), spread_first)
     give(2, 1)
     take(2)
     close(2, ((q_b, kv_b, pair),), spread_last)
@@ -423,6 +449,8 @@
     def send_halo(c):
         sp_copy(kv_b.at[c, :, pl.ds(sub - halo_sub, halo_sub), :], halo.at[c], sent, hr, above).start()
 
+    take(4)
+
     @pl.when(s < n - 1)
     def _():
         send_halo(two)
@@ -432,8 +460,15 @@
     def _():
         send_halo(pair)
 
+    close(4, ((q_b, kv_b, mirror),), lambda: None)
+
+    @pl.when((s < n - 1) & (s != 1))
+    def _():
+        send_halo(mirror)
+
     cross(1)
     prod, more = add_mirror(xp)
+    take(5)
     same(tp_copy, hm.at[diag], cfr, core).wait_recv()
     last, most = add_mirror(diag)
     finish(acc_m[...] + prod + last, squares[0] + more + most, tm[...], ((q_c, kv_c, mirror),), slice(0, sub))
@@ -447,19 +482,6 @@
         out = jnp.dot(weight.astype(bf16), v, preferred_element_type=f32) / total
         return out, top + jnp.log(total)
 
-    def log_count(*read):
-        count = sum(each.astype(f32) for each in read)
-        bias = jnp.where(count == 2, math.log(2.0), jnp.where(count == 3, math.log(3.0), 0.0))
-        return jnp.where(count == 0, -jnp.inf, bias)
-
-    def strided(behind, step):
-        return (behind >= 0) & (behind <= KEYS_BEHIND * step) & ((behind + rows * step) % step == 0)
-
-    later = (rows - sub, rows - sub)
-    late, early = iota(later, 0) + sub, iota(later, 1)
-    stride = WIDEST_DILATION // n
-    crosses = late // sub > early // sub
-    bias_c = log_count(strided(late - early, 1) & crosses, strided(late - early, stride) & crosses)
     lane = iota((rows, LANES), 1)
 
     def as_rows(columns):
@@ -477,59 +499,60 @@
         receive(2, h)
         receive(1, h)
         out, lse = attend(
-            flat(q_c[1:, h]), flat(kv_c[: n - 1, h, :, :hd]), flat(kv_c[: n - 1, h, :, hd:]), bias_c
+            flat(q_c[1:, h]), flat(kv_c[: n - 1, h, :, :hd]), flat(kv_c[: n - 1, h, :, hd:]), bias_far[...]
         )
+        lsend[h] = as_rows([None] + [lse[b * sub : (b + 1) * sub] for b in range(n - 1)])
+        rl[s, h] = lsend[h]
         oc[h, 1:] = out.astype(bf16).reshape(n - 1, sub, hd)
         for k in (3, 2, 1):
             @pl.when(peer[k] > 0)
             def _():
+                sp_copy(lsend.at[h], rl.at[s, h], sent, lr.at[k - 1, h], peer[k]).start()
                 sp_copy(oc.at[h, peer[k]], ro.at[s, h], sent, rr.at[k - 1, h], peer[k]).start()
-        lsend[h] = as_rows([None] + [lse[b * sub : (b + 1) * sub] for b in range(n - 1)])
-        rl[s, h] = lsend[h]
-        for k in (3, 2, 1):
-            @pl.when(peer[k] > 0)
-            def _():
-                sp_copy(lsend.at[h], rl.at[s, h], sent, lr.at[k - 1, h], peer[k]).start()
+
+    wf = []
+
+    def pass_on(j):
+        piece = wo.at[(xp, diag)[j // 2], quarter_of(j % 2)]
+        w_sends[j + 1].wait_recv()
+        wf.append(go(copy_to("grp", piece, piece, sent, wfr.at[j], 1 - g)))
 
     far_head(0)
-    take(4)
-    close(4, ((q_b, kv_b, mirror),), lambda: None)
-
-    @pl.when((s < n - 1) & (s != 1))
-    def _():
-        send_halo(mirror)
-
     for h in range(1, heads):
         far_head(h)
-
-    wf = []
-
-    def pass_on(j):
-        q = (xp, diag)[j]
-        w_sends[j + 1].wait_recv()
-        wf.append(go(copy_to("grp", wo.at[q, mine], wo.at[q, mine], sent, wfr.at[j], 1 - g)))
-
     pass_on(0)
-
-    behind = row_of(iota(square, 0), sub) - row_of(iota(square, 1), sub)
-    bias_b = log_count(*(strided(behind, step) for step in (1, n, WIDEST_DILATION)))
-    gx = [same(tp_copy, at.at[p, h], gxr.at[h], xp) for h in range(heads)]
-    gc = [same(tp_copy, at.at[p, h], gcr, core) for h in range(heads)]
-
-    def share(h):
-        gx[h].start()
-        gc[h].start()
+    close(5, ((q_b, kv_b, mirror),), lambda: None)
+    pass_on(1)
+
+    others = pl.ds(0, n - 1)
+    gx = [same(tp_copy, at.at[p, h, others], gxr.at[h], xp) for h in range(heads)]
+    gc = [same(tp_copy, at.at[p, h, others], gcr, core) for h in range(heads)]
+    gx.append(same(tp_copy, at_own.at[p], gxr.at[heads], xp))
+    gc.append(same(tp_copy, at_own.at[p], gor, core))
+
+    def share(j):
+        gx[j].start()
+        gc[j].start()
+
+    def slot(c):
+        return lax.rem(lax.rem(c + s, 2) + 2 * lax.rem(c // 2 + s // 2, 2) + n - 1, n)
 
     for h in range(heads):
-        out, lse = attend(flat(q_b[:, h]), flat(kv_b[:, h, :, :hd]), flat(kv_b[:, h, :, hd:]), bias_b)
+        out, lse = attend(flat(q_b[:, h]), flat(kv_b[:, h, :, :hd]), flat(kv_b[:, h, :, hd:]), bias_near[...])
         near_out[h] = out.reshape(n, sub, hd)
         near_row[h] = as_rows([lse[c * sub : (c + 1) * sub] for c in range(n)])
 
         @pl.when(s == 0)
         def _():
-            at[p, h] = near_out[h].astype(bf16)
+            at_own[p, h] = near_out[h, 0].astype(bf16)
+            for c in range(1, n):
+                at[p, h, c - 1] = near_out[h, c].astype(bf16)
+            if h == heads - 1:
+                share(heads)
             share(h)
             all_log[h] = near_row[h]
+
+        pass_on(2 + h)
 
     @pl.when(s > 0)
     def _():
@@ -548,44 +571,67 @@
                 jnp.concatenate([lse[c * halo_sub : (c + 1) * halo_sub], pad], axis=0) for c in range(n)
             ])
 
-    pass_on(1)
+    which = iota((8, LANES), 0)
+
+    def weigh(own, low, far_row):
+        top = jnp.maximum(jnp.maximum(own, low), far_row)
+        exps = [jnp.exp(x - top) for x in (own, low, far_row)]
+        both = exps[0] + exps[1] + exps[2]
+        return [x / both for x in exps], top + jnp.log(both)
+
+    def as_columns(shares):
+        pad = jnp.zeros((LANES - 8 * len(shares), LANES), f32)
+        return jnp.transpose(jnp.concatenate(shares + [pad], axis=0))[:sub]
+
+    def blend(parts, own, far_out, low):
+        sums = parts[0] * own + parts[2] * far_out.astype(f32)
+        return jnp.concatenate([sums[:halo_sub] + parts[1][:halo_sub] * low, sums[halo_sub:]], axis=0).astype(bf16)
 
     @pl.when(s > 0)
     def _():
+        mine = pl.ds(s, 1)
+        rows_of = jnp.zeros((8, LANES), f32)
         for h in range(heads):
+            shares, _ = weigh(near_row[h, mine], halo_row[h, mine], rl[s, h, mine])
+            for j, x in enumerate(shares):
+                rows_of = jnp.where(which == 3 * h + j, x, rows_of)
+        columns = as_columns([rows_of])
+        for h in range(heads):
+            parts = [columns[:, 3 * h + j : 3 * h + j + 1] for j in range(3)]
+            at_own[p, h] = blend(parts, near_out[h, s], oc[h, s], halo_out[h, s])
+        share(heads)
+        for h in range(heads):
+            ro[s, h] = oc[h, s]
             for k in (1, 2, 3):
+                same(sp_copy, rl.at[peer[k], h], lr.at[k - 1, h], peer[k]).wait_recv()
                 same(sp_copy, ro.at[peer[k], h], rr.at[k - 1, h], peer[k]).wait_recv()
-                same(sp_copy, rl.at[peer[k], h], lr.at[k - 1, h], peer[k]).wait_recv()
-            ro[s, h] = oc[h, s]
-            which = iota((8, LANES), 0)
-            far_row = jnp.full((8, LANES), -jnp.inf, f32)
+            far_row = jnp.zeros((8, LANES), f32)
             for c in range(n):
-                far_row = jnp.where(which == c, rl[c, h, pl.ds(s, 1), :], far_row)
-            own, low = near_row[h], halo_row[h]
-            live = (which < n) & (iota((8, LANES), 1) < sub)
-            top = jnp.where(live, jnp.maximum(jnp.maximum(own, low), far_row), 0.0)
-            exps = [jnp.where(live, jnp.exp(x - top), 0.0) for x in (own, low, far_row)]
-            both = jnp.where(live, exps[0] + exps[1] + exps[2], 1.0)
-            all_log[h] = top + jnp.log(both)
-            shares = [x / both for x in exps]
-            columns = jnp.transpose(jnp.concatenate(shares + [jnp.zeros((LANES - 24, LANES), f32)], axis=0))[:sub]
+                far_row = jnp.where(which == c, rl[c, h, mine], far_row)
+            live = which < n
+            shares, all_log[h] = weigh(*(jnp.where(live, x, 0.0) for x in (near_row[h], halo_row[h], far_row)))
+            columns = as_columns(shares)
             for c in range(n):
-                own_part = columns[:, c : c + 1] * near_out[h, c]
-                far_part = columns[:, 16 + c : 17 + c] * ro[c, h].astype(f32)
-                low_part = columns[:halo_sub, 8 + c : 9 + c] * halo_out[h, c]
-                sums = own_part + far_part
-                sums = jnp.concatenate([sums[:halo_sub] + low_part, sums[halo_sub:]], axis=0)
-                at[p, h, c] = sums.astype(bf16)
+                parts = [columns[:, 8 * j + c : 8 * j + c + 1] for j in range(3)]
+                at[p, h, slot(c)] = blend(parts, near_out[h, c], ro[c, h], halo_out[h, c])
             share(h)
 
-    from_class = (iota(square, 0) == row_of(iota(square, 1), sub)).astype(f32).astype(bf16)
+    block = iota(square, 1) // sub
+    class_of = jnp.where(block == 0, pair, jnp.where(block == 1, two, jnp.where(block == 2, mirror, s)))
+    from_class = (iota(square, 0) == n * lax.rem(iota(square, 1), sub) + class_of).astype(f32).astype(bf16)
+
     def product(q):
-        x = jnp.concatenate([flat(at[q, h]) for h in range(heads)], axis=1)
+        x = jnp.concatenate([
+            jnp.concatenate([flat(at[q, h, : n - 1]), at_own[q, h]], axis=0) for h in range(heads)
+        ], axis=1)
         return jnp.dot(x, wo[q], preferred_element_type=f32)
 
-    def forward(h):
-        gx[h].wait_recv()
-        go(same(tp_copy, at.at[xp, h], gfr, core))
+    def forward(j):
+        gx[j].wait_recv()
+        if j == heads:
+            go(same(tp_copy, at_own.at[xp], gpr, core))
+        else:
+            go(same(tp_copy, at.at[xp, j, others], gfr, core))
 
     by_head = iota((8, LANES), 0)
     logs = []
@@ -608,16 +654,18 @@
     total_ref[...] = total[:heads]
 
     result = product(p)
-    forward(0)
+    forward(heads)
     w_sends[0].wait_recv()
-    same(tp_copy, at.at[core], gcr, core).wait_recv()
+    same(tp_copy, at_own.at[core], gor, core).wait_recv()
+    same(tp_copy, at.at[core, :, others], gcr, core).wait_recv()
     result += product(core)
-    for h in range(1, heads):
+    for h in range(heads):
         forward(h)
     for copy in wf:
         copy.wait_recv()
     result += product(xp)
-    same(tp_copy, at.at[diag], gfr, core).wait_recv()
+    same(tp_copy, at_own.at[diag], gpr, core).wait_recv()
+    same(tp_copy, at.at[diag, :, others], gfr, core).wait_recv()
     result += product(diag)
     mixed_ref[...] = jnp.dot(from_class, result.astype(bf16), preferred_element_type=f32).astype(bf16)
     back = heads * (sub * hd * 2 + 8 * LANES * 4)
@@ -639,6 +687,17 @@
     @pl.when(s == n - 1)
     def _():
         all_sent(sum(sends) + at_bytes + q_bytes + 2 * back)
+
+
+def write_kernel(mixed_ref, total_ref, out_ref, log_ref, sems):
+    copies = [
+        pltpu.make_async_copy(mixed_ref, out_ref, sems.at[0]),
+        pltpu.make_async_copy(total_ref, log_ref, sems.at[1]),
+    ]
+    for copy in copies:
+        copy.start()
+    for copy in copies:
+        copy.wait()
 
 
 def local_by_class(hidden, norm_gain, w_query, w_key, w_value, query_gain, key_gain, w_out):
@@ -691,11 +750,14 @@
             pltpu.VMEM((heads, 8, LANES), f32),
             pltpu.VMEM((heads, 8, LANES), f32),
             pltpu.VMEM((4, heads, n, sub, hd), bf16),
+            pltpu.VMEM((4, heads, sub, hd), bf16),
+            pltpu.VMEM((rows - sub, rows - sub), f32),
+            pltpu.VMEM((rows, rows), f32),
             pltpu.VMEM((4, 1, width), f32),
             pltpu.VMEM((most_bytes // (4 * LANES), LANES), f32),
-            dma((10,)), dma, dma((2,)), dma((n + 1,)), dma, dma((n + 1,)), dma((2,)), dma, dma,
-            dma((3,)), dma((2,)), dma((2, heads, 2)), dma((2, heads, 2)), dma, dma((3, heads)), dma((3, heads)),
-            dma((heads,)), dma, dma,
+            dma((10,)), dma, dma((2,)), dma((n + 2,)), dma, dma((n + 2,)), dma((2,)), dma, dma,
+            dma((5,)), dma((4,)), dma((2, heads, 2)), dma((2, heads, 2)), dma, dma((3, heads)), dma((3, heads)),
+            dma((heads + 1,)), dma, dma, dma, dma,
         ],
         compiler_params=pltpu.CompilerParams(
             collective_id=0, has_side_effects=True, vmem_limit_bytes=60 * 1024 * 1024
@@ -703,6 +765,18 @@
     )(
         hidden, norm_gain.reshape(-1, LANES), query_gain, key_gain,
         w_query, w_key, w_value, w_out, table,
+    )
+    mixed, total = pl.pallas_call(
+        write_kernel,
+        out_shape=(
+            jax.ShapeDtypeStruct(mixed.shape, bf16), jax.ShapeDtypeStruct(total.shape, f32)
+        ),
+        in_specs=[vmem, vmem],
+        out_specs=(anyspace, anyspace),
+        scratch_shapes=[dma((2,))],
+    )(
+        pltpu.with_memory_space_constraint(mixed, pltpu.VMEM),
+        pltpu.with_memory_space_constraint(total, pltpu.VMEM),
     )
     return mixed, total.T
 

time: 33.8 us -> 31.7 us (0.938)
  the two profiles are of different devices: /device:TPU:31 before, /device:TPU:0 now
where the time goes in v3:
time: 31.7 us; the launch traced here: 31.1 us
  Pallas kernels  30.4 us (96%)
  between operations  0.64 us (2%)
    pallas_call x1, Pallas kernels, local_by_class(): pl.pallas_call(class_kernel, out_shape=(pltpu.VMEM((rows, w_out.shape[1]...  29.6 us
    pallas_call x1, Pallas kernels, local_by_class(): pl.pallas_call(write_kernel, out_shape=(jax.ShapeDtypeStruct(mixed.shape,...  0.77 us

profile of v3, /device:TPU:0, one launch (start us, length us, event | category | flops | bytes accessed | tf_op | source)
XLA Modules:
  0.0 31.1 jit_solution(6986753766184000174)
XLA Ops:
  0.6 29.6 %shard_map.104 = (bf16[384,512]{1,0:T(8,128)(2,1)S(1)}, f32[2,384]{1,0:T(2,128)S(1)}) custom-call(bf16[384,512]{1,0:T(8,128)(2,1)} %hid_ref.1, bf16[16,128]{1,0:T(8,128)(2,1)} %bitcast.2, f32[2,128]{1,0:T(2,128)} %qgain_ref.1, f32[2,128]{1,0:T(2,128)} %kgain_ref.1, bf16[2048,256]{1,0:T(8,128)(2,1)} %wq_ref.1, bf16[2048,256]{1,0:T(8,128)(2,1)} %wk_ref.1, ...), custom_call_target="tpu_custom_call" | custom-call | tf_op jit(solution)/shard_map/pallas_call | solution.py:716
  30.3 0.8 %shard_map.105 = (bf16[384,512]{1,0:T(8,128)(2,1)}, f32[2,384]{1,0:T(2,128)}) custom-call(bf16[384,512]{1,0:T(8,128)(2,1)S(1)} %get-tuple-element.6.mixed_ref, f32[2,384]{1,0:T(2,128)S(1)} %get-tuple-element.7.total_ref), custom_call_target="tpu_custom_call" | custom-call | tf_op jit(solution)/shard_map/pallas_call | solution.py:769

commit v4 on v3

--- a/solution.py
+++ b/solution.py
@@ -525,17 +525,21 @@
     pass_on(1)
 
     others = pl.ds(0, n - 1)
-    gx = [same(tp_copy, at.at[p, h, others], gxr.at[h], xp) for h in range(heads)]
-    gc = [same(tp_copy, at.at[p, h, others], gcr, core) for h in range(heads)]
-    gx.append(same(tp_copy, at_own.at[p], gxr.at[heads], xp))
-    gc.append(same(tp_copy, at_own.at[p], gor, core))
+
+    def pair_of(piece, j, near_sem):
+        return same(tp_copy, piece, gxr.at[j], xp), same(tp_copy, piece, near_sem, core)
+
+    def index(k, h):
+        return 1 + h * (n - 1) + k - 1
+
+    shared = [pair_of(at_own.at[p], 0, gor)]
+    for h in range(heads):
+        for k in range(1, n):
+            shared.append(pair_of(at.at[p, h, k - 1], index(k, h), gcr))
 
     def share(j):
-        gx[j].start()
-        gc[j].start()
-
-    def slot(c):
-        return lax.rem(lax.rem(c + s, 2) + 2 * lax.rem(c // 2 + s // 2, 2) + n - 1, n)
+        for copy in shared[j]:
+            copy.start()
 
     for h in range(heads):
         out, lse = attend(flat(q_b[:, h]), flat(kv_b[:, h, :, :hd]), flat(kv_b[:, h, :, hd:]), bias_near[...])
@@ -548,11 +552,12 @@
             for c in range(1, n):
                 at[p, h, c - 1] = near_out[h, c].astype(bf16)
             if h == heads - 1:
-                share(heads)
-            share(h)
+                share(0)
+            for k in range(1, n):
+                share(index(k, h))
             all_log[h] = near_row[h]
 
-        pass_on(2 + h)
+    pass_on(2)
 
     @pl.when(s > 0)
     def _():
@@ -587,34 +592,35 @@
         sums = parts[0] * own + parts[2] * far_out.astype(f32)
         return jnp.concatenate([sums[:halo_sub] + parts[1][:halo_sub] * low, sums[halo_sub:]], axis=0).astype(bf16)
 
+    mine = pl.ds(s, 1)
+
+    def merge(c, hs):
+        row = pl.ds(c, 1)
+        rows_of = jnp.zeros((8, LANES), f32)
+        for i, h in enumerate(hs):
+            shares, all_log[h, row] = weigh(near_row[h, row], halo_row[h, row], rl[c, h, mine])
+            for j, x in enumerate(shares):
+                rows_of = jnp.where(which == 3 * i + j, x, rows_of)
+        columns = as_columns([rows_of])
+        return [[columns[:, 3 * i + j : 3 * i + j + 1] for j in range(3)] for i in range(len(hs))]
+
     @pl.when(s > 0)
     def _():
-        mine = pl.ds(s, 1)
-        rows_of = jnp.zeros((8, LANES), f32)
+        for h, parts in enumerate(merge(s, range(heads))):
+            at_own[p, h] = blend(parts, near_out[h, s], oc[h, s], halo_out[h, s])
+        share(0)
+
+    pass_on(3)
+
+    @pl.when(s > 0)
+    def _():
         for h in range(heads):
-            shares, _ = weigh(near_row[h, mine], halo_row[h, mine], rl[s, h, mine])
-            for j, x in enumerate(shares):
-                rows_of = jnp.where(which == 3 * h + j, x, rows_of)
-        columns = as_columns([rows_of])
-        for h in range(heads):
-            parts = [columns[:, 3 * h + j : 3 * h + j + 1] for j in range(3)]
-            at_own[p, h] = blend(parts, near_out[h, s], oc[h, s], halo_out[h, s])
-        share(heads)
-        for h in range(heads):
-            ro[s, h] = oc[h, s]
-            for k in (1, 2, 3):
-                same(sp_copy, rl.at[peer[k], h], lr.at[k - 1, h], peer[k]).wait_recv()
-                same(sp_copy, ro.at[peer[k], h], rr.at[k - 1, h], peer[k]).wait_recv()
-            far_row = jnp.zeros((8, LANES), f32)
-            for c in range(n):
-                far_row = jnp.where(which == c, rl[c, h, mine], far_row)
-            live = which < n
-            shares, all_log[h] = weigh(*(jnp.where(live, x, 0.0) for x in (near_row[h], halo_row[h], far_row)))
-            columns = as_columns(shares)
-            for c in range(n):
-                parts = [columns[:, 8 * j + c : 8 * j + c + 1] for j in range(3)]
-                at[p, h, slot(c)] = blend(parts, near_out[h, c], ro[c, h], halo_out[h, c])
-            share(h)
+            for k in range(1, n):
+                c = peer[k]
+                same(sp_copy, rl.at[c, h], lr.at[k - 1, h], c).wait_recv()
+                same(sp_copy, ro.at[c, h], rr.at[k - 1, h], c).wait_recv()
+                at[p, h, k - 1] = blend(merge(c, (h,))[0], near_out[h, c], ro[c, h], halo_out[h, c])
+                share(index(k, h))
 
     block = iota(square, 1) // sub
     class_of = jnp.where(block == 0, pair, jnp.where(block == 1, two, jnp.where(block == 2, mirror, s)))
@@ -627,11 +633,11 @@
         return jnp.dot(x, wo[q], preferred_element_type=f32)
 
     def forward(j):
-        gx[j].wait_recv()
-        if j == heads:
+        shared[j][0].wait_recv()
+        if j == 0:
             go(same(tp_copy, at_own.at[xp], gpr, core))
         else:
-            go(same(tp_copy, at.at[xp, j, others], gfr, core))
+            go(same(tp_copy, at.at[xp, (j - 1) // (n - 1), (j - 1) % (n - 1)], gfr, core))
 
     by_head = iota((8, LANES), 0)
     logs = []
@@ -654,13 +660,12 @@
     total_ref[...] = total[:heads]
 
     result = product(p)
-    forward(heads)
+    for j in (*range(1, n), 0, *range(n, len(shared))):
+        forward(j)
     w_sends[0].wait_recv()
     same(tp_copy, at_own.at[core], gor, core).wait_recv()
     same(tp_copy, at.at[core, :, others], gcr, core).wait_recv()
     result += product(core)
-    for h in range(heads):
-        forward(h)
     for copy in wf:
         copy.wait_recv()
     result += product(xp)
@@ -757,7 +762,7 @@
             pltpu.VMEM((most_bytes // (4 * LANES), LANES), f32),
             dma((10,)), dma, dma((2,)), dma((n + 2,)), dma, dma((n + 2,)), dma((2,)), dma, dma,
             dma((5,)), dma((4,)), dma((2, heads, 2)), dma((2, heads, 2)), dma, dma((3, heads)), dma((3, heads)),
-            dma((heads + 1,)), dma, dma, dma, dma,
+            dma((1 + 3 * heads,)), dma, dma, dma, dma,
         ],
         compiler_params=pltpu.CompilerParams(
             collective_id=0, has_side_effects=True, vmem_limit_bytes=60 * 1024 * 1024

time: 31.7 us -> 31.2 us (0.984); the launches traced: 31.1 us -> 31.1 us
  no operation moved by 1% of the time
where the time goes in v4:
time: 31.2 us; the launch traced here: 31.1 us
  Pallas kernels  30.4 us (97%)
  between operations  0.64 us (2%)
    pallas_call x1, Pallas kernels, local_by_class(): pl.pallas_call(class_kernel, out_shape=(pltpu.VMEM((rows, w_out.shape[1]...  29.7 us
    pallas_call x1, Pallas kernels, local_by_class(): pl.pallas_call(write_kernel, out_shape=(jax.ShapeDtypeStruct(mixed.shape,...  0.77 us

profile of v4, /device:TPU:0, one launch (start us, length us, event | category | flops | bytes accessed | tf_op | source)
XLA Modules:
  0.0 31.1 jit_solution(16035234279711420012)
XLA Ops:
  0.6 29.7 %shard_map.104 = (bf16[384,512]{1,0:T(8,128)(2,1)S(1)}, f32[2,384]{1,0:T(2,128)S(1)}) custom-call(bf16[384,512]{1,0:T(8,128)(2,1)} %hid_ref.1, bf16[16,128]{1,0:T(8,128)(2,1)} %bitcast.2, f32[2,128]{1,0:T(2,128)} %qgain_ref.1, f32[2,128]{1,0:T(2,128)} %kgain_ref.1, bf16[2048,256]{1,0:T(8,128)(2,1)} %wq_ref.1, bf16[2048,256]{1,0:T(8,128)(2,1)} %wk_ref.1, ...), custom_call_target="tpu_custom_call" | custom-call | tf_op jit(solution)/shard_map/pallas_call | solution.py:721
  30.3 0.8 %shard_map.105 = (bf16[384,512]{1,0:T(8,128)(2,1)}, f32[2,384]{1,0:T(2,128)}) custom-call(bf16[384,512]{1,0:T(8,128)(2,1)S(1)} %get-tuple-element.6.mixed_ref, f32[2,384]{1,0:T(2,128)S(1)} %get-tuple-element.7.total_ref), custom_call_target="tpu_custom_call" | custom-call | tf_op jit(solution)/shard_map/pallas_call | solution.py:774

commit v5 on v4

--- a/solution.py
+++ b/solution.py
@@ -197,7 +197,7 @@
     mixed_ref, total_ref,
     hid, gain_in, qgain, kgain, hb, hm, wall, wo, tb, tm, acc, acc_m, sq, q_b, kv_b, q_c, kv_c,
     halo, oc, lsend, ro, rl, near_out, near_row, halo_out, halo_row, all_log, at, at_own, bias_far, bias_near, gain, drain,
-    loc, sent, zr, axr, acr, afr, cxr, ccr, cfr, wor, wfr, qr, kr, hr, rr, lr, gxr, gcr, gfr, gor, gpr,
+    loc, sent, zr, axr, acr, afr, cxr, ccr, cfr, wor, wfr, wzr, qr, kr, hr, rr, lr, gxr, gcr, gfr, gor, gpr,
 ):
     f32, bf16 = jnp.float32, jnp.bfloat16
     g, s, p = lax.axis_index("grp"), lax.axis_index("sp"), lax.axis_index("tp")
@@ -281,9 +281,10 @@
     for copy in ax[:4]:
         go(copy)
     ac = go(same(tp_copy, hb.at[p], acr, core))
-    w_sends = [
-        go(tp_copy(wo_ref.at[:, pl.ds(pl.multiple_of(core * width, LANES), width)], wo.at[p], sent, wor.at[0], core))
-    ]
+    w_core = go(tp_copy(
+        wo_ref.at[:, pl.ds(pl.multiple_of(core * width, LANES), width)],
+        wo.at[p], sent, wor.at[0], core,
+    ))
 
     for load in loads:
         load.wait()
@@ -388,6 +389,13 @@
     def quarter_of(a):
         return pl.ds(pl.multiple_of((2 * g + a) * quarter, 8), quarter)
 
+    def w_copy(i):
+        q, block = (xp, diag)[i // 2], quarter_of(i % 2)
+        source = wo_ref.at[block, pl.ds(pl.multiple_of(q * width, LANES), width)]
+        return tp_copy(source, wo.at[p, block], sent, wor.at[1 + i], q)
+
+    w_copies = [w_copy(i) for i in range(4)]
+
     def spread_first():
         spread(0)
         go(ax[4])
@@ -395,13 +403,12 @@
     def spread_last():
         spread(1)
         go(ax[5])
-        for j, q in ((0, xp), (1, diag)):
-            for a in range(2):
-                block = quarter_of(a)
-                w_sends.append(go(tp_copy(
-                    wo_ref.at[block, pl.ds(pl.multiple_of(q * width, LANES), width)], wo.at[p, block],
-                    sent, wor.at[1 + 2 * j + a], q,
-                )))
+        @pl.when(s > 0)
+        def _():
+            w_copies[3].start()
+
+        for copy in w_copies[:3]:
+            go(copy)
 
     def add_mirror(q):
         prod, more = chunk(hm[q].reshape(sub, width), q)
@@ -510,19 +517,38 @@
                 sp_copy(lsend.at[h], rl.at[s, h], sent, lr.at[k - 1, h], peer[k]).start()
                 sp_copy(oc.at[h, peer[k]], ro.at[s, h], sent, rr.at[k - 1, h], peer[k]).start()
 
-    wf = []
-
-    def pass_on(j):
-        piece = wo.at[(xp, diag)[j // 2], quarter_of(j % 2)]
-        w_sends[j + 1].wait_recv()
-        wf.append(go(copy_to("grp", piece, piece, sent, wfr.at[j], 1 - g)))
+
+    def y_copy(i):
+        piece = wo.at[(xp, diag)[i // 2], quarter_of(i % 2)]
+        return copy_to("grp", piece, piece, sent, wfr.at[i], 1 - g)
+
+    def pass_step(i):
+        later = (i + 3) % 4
+
+        @pl.when(s > 0)
+        def _():
+            w_copies[later].wait_recv()
+            y_copy(later).start()
+
+        if i == 0:
+            @pl.when(s == 1)
+            def _():
+                same(sp_copy, wo.at[diag, quarter_of(1)], wzr, s - 1).start()
+
+        @pl.when(s == 0)
+        def _():
+            if i < 3:
+                w_copies[i].wait_recv()
+            else:
+                same(sp_copy, wo.at[diag, quarter_of(1)], wzr, s + 1).wait_recv()
+            y_copy(i).start()
 
     far_head(0)
+    pass_step(0)
     for h in range(1, heads):
         far_head(h)
-    pass_on(0)
+    pass_step(1)
     close(5, ((q_b, kv_b, mirror),), lambda: None)
-    pass_on(1)
 
     others = pl.ds(0, n - 1)
 
@@ -557,7 +583,7 @@
                 share(index(k, h))
             all_log[h] = near_row[h]
 
-    pass_on(2)
+    pass_step(2)
 
     @pl.when(s > 0)
     def _():
@@ -566,17 +592,18 @@
         small = (halo_rows, halo_rows)
         behind = row_of(iota(small, 0), halo_sub) - row_of(iota(small, 1), halo_sub) + halo_rows
         bias_h = jnp.where(behind <= KEYS_BEHIND, 0.0, -jnp.inf).astype(f32)
+        low = []
+        pad = jnp.full((sub - halo_sub, 1), -jnp.inf, f32)
         for h in range(heads):
             out, lse = attend(
                 flat(q_b[:, h, :halo_sub]), flat(halo[:, h, :, :hd]), flat(halo[:, h, :, hd:]), bias_h
             )
             halo_out[h] = out.reshape(n, halo_sub, hd)
-            pad = jnp.full((sub - halo_sub, 1), -jnp.inf, f32)
-            halo_row[h] = as_rows([
-                jnp.concatenate([lse[c * halo_sub : (c + 1) * halo_sub], pad], axis=0) for c in range(n)
-            ])
-
-    which = iota((8, LANES), 0)
+            for c in range(n):
+                low.append(jnp.concatenate([lse[c * halo_sub : (c + 1) * halo_sub], pad], axis=0))
+        halo_row[...] = as_rows(low)
+
+    which = iota((16, LANES), 0)
 
     def weigh(own, low, far_row):
         top = jnp.maximum(jnp.maximum(own, low), far_row)
@@ -585,7 +612,7 @@
         return [x / both for x in exps], top + jnp.log(both)
 
     def as_columns(shares):
-        pad = jnp.zeros((LANES - 8 * len(shares), LANES), f32)
+        pad = jnp.zeros((LANES - 16 * len(shares), LANES), f32)
         return jnp.transpose(jnp.concatenate(shares + [pad], axis=0))[:sub]
 
     def blend(parts, own, far_out, low):
@@ -594,33 +621,37 @@
 
     mine = pl.ds(s, 1)
 
-    def merge(c, hs):
-        row = pl.ds(c, 1)
-        rows_of = jnp.zeros((8, LANES), f32)
-        for i, h in enumerate(hs):
-            shares, all_log[h, row] = weigh(near_row[h, row], halo_row[h, row], rl[c, h, mine])
+    def merge(places):
+        rows_of = jnp.zeros((16, LANES), f32)
+        for i, (c, h) in enumerate(places):
+            row = pl.ds(c, 1)
+            shares, all_log[h, row] = weigh(near_row[h, row], halo_row[pl.ds(h * n + c, 1)], rl[c, h, mine])
             for j, x in enumerate(shares):
                 rows_of = jnp.where(which == 3 * i + j, x, rows_of)
         columns = as_columns([rows_of])
-        return [[columns[:, 3 * i + j : 3 * i + j + 1] for j in range(3)] for i in range(len(hs))]
+        for i, (c, h) in enumerate(places):
+            parts = [columns[:, 3 * i + j : 3 * i + j + 1] for j in range(3)]
+            yield lambda far, c=c, h=h, parts=parts: blend(parts, near_out[h, c], far[...], halo_out[h, c])
 
     @pl.when(s > 0)
     def _():
-        for h, parts in enumerate(merge(s, range(heads))):
-            at_own[p, h] = blend(parts, near_out[h, s], oc[h, s], halo_out[h, s])
+        for h, mixed in enumerate(merge([(s, h) for h in range(heads)])):
+            at_own[p, h] = mixed(oc.at[h, s])
         share(0)
 
-    pass_on(3)
+    pass_step(3)
 
     @pl.when(s > 0)
     def _():
         for h in range(heads):
-            for k in range(1, n):
-                c = peer[k]
-                same(sp_copy, rl.at[c, h], lr.at[k - 1, h], c).wait_recv()
-                same(sp_copy, ro.at[c, h], rr.at[k - 1, h], c).wait_recv()
-                at[p, h, k - 1] = blend(merge(c, (h,))[0], near_out[h, c], ro[c, h], halo_out[h, c])
-                share(index(k, h))
+            for ks in ((1,), (2, 3)) if h < heads - 1 else ((1,), (2, 3)):
+                for k in ks:
+                    same(sp_copy, rl.at[peer[k], h], lr.at[k - 1, h], peer[k]).wait_recv()
+                    same(sp_copy, ro.at[peer[k], h], rr.at[k - 1, h], peer[k]).wait_recv()
+                for k, mixed in zip(ks, merge([(peer[k], h) for k in ks])):
+                    at[p, h, k - 1] = mixed(ro.at[peer[k], h])
+                for k in ks:
+                    share(index(k, h))
 
     block = iota(square, 1) // sub
     class_of = jnp.where(block == 0, pair, jnp.where(block == 1, two, jnp.where(block == 2, mirror, s)))
@@ -662,12 +693,12 @@
     result = product(p)
     for j in (*range(1, n), 0, *range(n, len(shared))):
         forward(j)
-    w_sends[0].wait_recv()
+    w_core.wait_recv()
     same(tp_copy, at_own.at[core], gor, core).wait_recv()
     same(tp_copy, at.at[core, :, others], gcr, core).wait_recv()
     result += product(core)
-    for copy in wf:
-        copy.wait_recv()
+    for i in range(4):
+        y_copy(i).wait_recv()
     result += product(xp)
     same(tp_copy, at_own.at[diag], gpr, core).wait_recv()
     same(tp_copy, at.at[diag, :, others], gfr, core).wait_recv()
@@ -677,21 +708,28 @@
     q_bytes, kv_bytes = 2 * heads * sub * hd * 2, 2 * heads * sub * 2 * hd * 2
     halo_bytes = (n - 1) * heads * halo_sub * 2 * hd * 2
     at_bytes = 2 * rows * lw * 2
+    w_bytes = quarter * width * 2
 
     def all_sent(total):
         same(tp_copy, drain.at[pl.ds(0, total // (LANES * 4))], acr, core).wait_send()
 
+    always = sum(sends) + at_bytes + 4 * w_bytes + 2 * back
+
     @pl.when(s == 0)
     def _():
-        all_sent(sum(sends) + at_bytes + kv_bytes + halo_bytes + 3 * back)
-
-    @pl.when((s > 0) & (s < n - 1))
-    def _():
-        all_sent(sum(sends) + at_bytes + q_bytes + kv_bytes + halo_bytes + 2 * back)
+        all_sent(always + kv_bytes + halo_bytes + back)
+
+    @pl.when(s == 1)
+    def _():
+        all_sent(always + q_bytes + kv_bytes + halo_bytes + 2 * w_bytes)
+
+    @pl.when((s > 1) & (s < n - 1))
+    def _():
+        all_sent(always + q_bytes + kv_bytes + halo_bytes + w_bytes)
 
     @pl.when(s == n - 1)
     def _():
-        all_sent(sum(sends) + at_bytes + q_bytes + 2 * back)
+        all_sent(always + q_bytes + w_bytes)
 
 
 def write_kernel(mixed_ref, total_ref, out_ref, log_ref, sems):
@@ -752,7 +790,7 @@
             pltpu.VMEM((heads, n, sub, hd), f32),
             pltpu.VMEM((heads, 8, LANES), f32),
             pltpu.VMEM((heads, n, halo_sub, hd), f32),
-            pltpu.VMEM((heads, 8, LANES), f32),
+            pltpu.VMEM((8, LANES), f32),
             pltpu.VMEM((heads, 8, LANES), f32),
             pltpu.VMEM((4, heads, n, sub, hd), bf16),
             pltpu.VMEM((4, heads, sub, hd), bf16),
@@ -761,7 +799,7 @@
             pltpu.VMEM((4, 1, width), f32),
             pltpu.VMEM((most_bytes // (4 * LANES), LANES), f32),
             dma((10,)), dma, dma((2,)), dma((n + 2,)), dma, dma((n + 2,)), dma((2,)), dma, dma,
-            dma((5,)), dma((4,)), dma((2, heads, 2)), dma((2, heads, 2)), dma, dma((3, heads)), dma((3, heads)),
+            dma((5,)), dma((4,)), dma, dma((2, heads, 2)), dma((2, heads, 2)), dma, dma((3, heads)), dma((3, heads)),
             dma((1 + 3 * heads,)), dma, dma, dma, dma,
         ],
         compiler_params=pltpu.CompilerParams(

time: 31.2 us -> 30.9 us (level)
  Pallas kernels: 30.4 us -> 29.8 us
    pallas_call x1, Pallas kernels: 29.7 us -> 29.1 us  [local_by_class(): pl.pallas_call(class_kernel, out_shape=(pltpu.VMEM((rows, w_out.shape[1]...]
where the time goes in v5:
time: 30.9 us; the launch traced here: 30.5 us
  Pallas kernels  29.8 us (96%)
  between operations  0.64 us (2%)
    pallas_call x1, Pallas kernels, local_by_class(): pl.pallas_call(class_kernel, out_shape=(pltpu.VMEM((rows, w_out.shape[1]...  29.1 us
    pallas_call x1, Pallas kernels, local_by_class(): pl.pallas_call(write_kernel, out_shape=(jax.ShapeDtypeStruct(mixed.shape,...  0.77 us

profile of v5, /device:TPU:0, one launch (start us, length us, event | category | flops | bytes accessed | tf_op | source)
XLA Modules:
  0.0 30.5 jit_solution(5981956668908098176)
XLA Ops:
  0.6 29.1 %shard_map.104 = (bf16[384,512]{1,0:T(8,128)(2,1)S(1)}, f32[2,384]{1,0:T(2,128)S(1)}) custom-call(bf16[384,512]{1,0:T(8,128)(2,1)} %hid_ref.1, bf16[16,128]{1,0:T(8,128)(2,1)} %bitcast.2, f32[2,128]{1,0:T(2,128)} %qgain_ref.1, f32[2,128]{1,0:T(2,128)} %kgain_ref.1, bf16[2048,256]{1,0:T(8,128)(2,1)} %wq_ref.1, bf16[2048,256]{1,0:T(8,128)(2,1)} %wk_ref.1, ...), custom_call_target="tpu_custom_call" | custom-call | tf_op jit(solution)/shard_map/pallas_call | solution.py:759
  29.7 0.8 %shard_map.105 = (bf16[384,512]{1,0:T(8,128)(2,1)}, f32[2,384]{1,0:T(2,128)}) custom-call(bf16[384,512]{1,0:T(8,128)(2,1)S(1)} %get-tuple-element.6.mixed_ref, f32[2,384]{1,0:T(2,128)S(1)} %get-tuple-element.7.total_ref), custom_call_target="tpu_custom_call" | custom-call | tf_op jit(solution)/shard_map/pallas_call | solution.py:812

commit v6 on v5

--- a/solution.py
+++ b/solution.py
@@ -278,7 +278,7 @@
         for a in range(2)
     ]
     ax = [same(tp_copy, hb.at[p, c, pl.ds(i, m), :], axr.at[j], xp) for j, (c, i, m) in enumerate(pieces)]
-    for copy in ax[:4]:
+    for copy in ax[:5]:
         go(copy)
     ac = go(same(tp_copy, hb.at[p], acr, core))
     w_core = go(tp_copy(
@@ -398,7 +398,6 @@
 
     def spread_first():
         spread(0)
-        go(ax[4])
 
     def spread_last():
         spread(1)
@@ -445,27 +444,30 @@
     take(1)
     close(1, ((q_b, kv_b, two),), spread_first)
     give(2, 1)
+    above = lax.rem(s + 1, n)
+
+    def send_halo(c):
+        sp_copy(kv_b.at[c, :, pl.ds(sub - halo_sub, halo_sub), :], halo.at[c], sent, hr, above).start()
+
+    @pl.when(s < n - 1)
+    def _():
+        send_halo(two)
+
     take(2)
     close(2, ((q_b, kv_b, pair),), spread_last)
     give(1, 0)
+    @pl.when(s == 1)
+    def _():
+        send_halo(pair)
+
     take(3)
     close(3, ((q_b, kv_b, s), (q_c, kv_c, s)), start_mirror)
 
-    above = lax.rem(s + 1, n)
-
-    def send_halo(c):
-        sp_copy(kv_b.at[c, :, pl.ds(sub - halo_sub, halo_sub), :], halo.at[c], sent, hr, above).start()
-
     take(4)
 
     @pl.when(s < n - 1)
     def _():
-        send_halo(two)
         send_halo(s)
-
-    @pl.when(s == 1)
-    def _():
-        send_halo(pair)
 
     close(4, ((q_b, kv_b, mirror),), lambda: None)
 

time: 30.9 us -> 30.6 us (level)
  no operation moved by 1% of the time
where the time goes in v6:
time: 30.6 us; the launch traced here: 30.5 us
  Pallas kernels  29.8 us (97%)
  between operations  0.64 us (2%)
    pallas_call x1, Pallas kernels, local_by_class(): pl.pallas_call(class_kernel, out_shape=(pltpu.VMEM((rows, w_out.shape[1]...  29.1 us
    pallas_call x1, Pallas kernels, local_by_class(): pl.pallas_call(write_kernel, out_shape=(jax.ShapeDtypeStruct(mixed.shape,...  0.77 us

profile of v6, /device:TPU:0, one launch (start us, length us, event | category | flops | bytes accessed | tf_op | source)
XLA Modules:
  0.0 30.5 jit_solution(4876550497042053541)
XLA Ops:
  0.6 29.1 %shard_map.104 = (bf16[384,512]{1,0:T(8,128)(2,1)S(1)}, f32[2,384]{1,0:T(2,128)S(1)}) custom-call(bf16[384,512]{1,0:T(8,128)(2,1)} %hid_ref.1, bf16[16,128]{1,0:T(8,128)(2,1)} %bitcast.2, f32[2,128]{1,0:T(2,128)} %qgain_ref.1, f32[2,128]{1,0:T(2,128)} %kgain_ref.1, bf16[2048,256]{1,0:T(8,128)(2,1)} %wq_ref.1, bf16[2048,256]{1,0:T(8,128)(2,1)} %wk_ref.1, ...), custom_call_target="tpu_custom_call" | custom-call | tf_op jit(solution)/shard_map/pallas_call | solution.py:761
  29.7 0.8 %shard_map.105 = (bf16[384,512]{1,0:T(8,128)(2,1)}, f32[2,384]{1,0:T(2,128)}) custom-call(bf16[384,512]{1,0:T(8,128)(2,1)S(1)} %get-tuple-element.6.mixed_ref, f32[2,384]{1,0:T(2,128)S(1)} %get-tuple-element.7.total_ref), custom_call_target="tpu_custom_call" | custom-call | tf_op jit(solution)/shard_map/pallas_call | solution.py:814

commit v7 on v6

--- a/solution.py
+++ b/solution.py
@@ -425,7 +425,7 @@
 
     def log_count(*read):
         count = sum(each.astype(f32) for each in read)
-        bias = jnp.where(count == 2, math.log(2.0), jnp.where(count == 3, math.log(3.0), 0.0))
+        bias = jnp.where(count == 2, 1.0, jnp.where(count == 3, math.log2(3.0), 0.0))
         return jnp.where(count == 0, -jnp.inf, bias)
 
     def strided(behind, step):
@@ -469,13 +469,12 @@
     def _():
         send_halo(s)
 
-    close(4, ((q_b, kv_b, mirror),), lambda: None)
+    close(4, ((q_b, kv_b, mirror),), functools.partial(cross, 1))
 
     @pl.when((s < n - 1) & (s != 1))
     def _():
         send_halo(mirror)
 
-    cross(1)
     prod, more = add_mirror(xp)
     take(5)
     same(tp_copy, hm.at[diag], cfr, core).wait_recv()
@@ -484,12 +483,12 @@
 
     def attend(q, k, v, bias):
         score = lax.dot_general(q, k, (((1,), (1,)), ((), ())), preferred_element_type=f32)
-        score = score * hd ** (-0.5) + bias
+        score = score * (hd ** (-0.5) / math.log(2.0)) + bias
         top = jnp.max(score, axis=-1, keepdims=True)
-        weight = jnp.exp(score - top)
+        weight = jnp.exp2(score - top)
         total = jnp.sum(weight, axis=-1, keepdims=True)
         out = jnp.dot(weight.astype(bf16), v, preferred_element_type=f32) / total
-        return out, top + jnp.log(total)
+        return out, top * math.log(2.0) + jnp.log(total)
 
     lane = iota((rows, LANES), 1)
 

time: 30.6 us -> 30.6 us (level)
  no operation moved by 1% of the time
where the time goes in v7:
time: 30.6 us; the launch traced here: 30.5 us
  Pallas kernels  29.8 us (97%)
  between operations  0.64 us (2%)
    pallas_call x1, Pallas kernels, local_by_class(): pl.pallas_call(class_kernel, out_shape=(pltpu.VMEM((rows, w_out.shape[1]...  29.1 us
    pallas_call x1, Pallas kernels, local_by_class(): pl.pallas_call(write_kernel, out_shape=(jax.ShapeDtypeStruct(mixed.shape,...  0.77 us

profile of v7, /device:TPU:0, one launch (start us, length us, event | category | flops | bytes accessed | tf_op | source)
XLA Modules:
  0.0 30.5 jit_solution(12652965882992093516)
XLA Ops:
  0.6 29.1 %shard_map.104 = (bf16[384,512]{1,0:T(8,128)(2,1)S(1)}, f32[2,384]{1,0:T(2,128)S(1)}) custom-call(bf16[384,512]{1,0:T(8,128)(2,1)} %hid_ref.1, bf16[16,128]{1,0:T(8,128)(2,1)} %bitcast.2, f32[2,128]{1,0:T(2,128)} %qgain_ref.1, f32[2,128]{1,0:T(2,128)} %kgain_ref.1, bf16[2048,256]{1,0:T(8,128)(2,1)} %wq_ref.1, bf16[2048,256]{1,0:T(8,128)(2,1)} %wk_ref.1, ...), custom_call_target="tpu_custom_call" | custom-call | tf_op jit(solution)/shard_map/pallas_call | solution.py:760
  29.7 0.8 %shard_map.105 = (bf16[384,512]{1,0:T(8,128)(2,1)}, f32[2,384]{1,0:T(2,128)}) custom-call(bf16[384,512]{1,0:T(8,128)(2,1)S(1)} %get-tuple-element.6.mixed_ref, f32[2,384]{1,0:T(2,128)S(1)} %get-tuple-element.7.total_ref), custom_call_target="tpu_custom_call" | custom-call | tf_op jit(solution)/shard_map/pallas_call | solution.py:813
